TPU v7x, 512 devices: a 4x2x32 block of a 4x8x32 slice. The times are simulated.
512 devices in a mesh: grp: 2 (over y), sp: 32 (over z), tp: 8 (over x, core).
Axes of the slice: x: 4, y: 2, z: 32, core: 2. Of those that a mesh axis runs over, the one named last changes fastest.
The devices are a block of a 4x8x32 slice.
Arguments:
- inputs: bfloat16 [16384, 2048], P(('grp', 'sp'), 'tp'), parts along dimension 0, may hold values from -20 to 20
- norm_gain: bfloat16 [2048], replicated, may hold values from 0.099609375 to 1.8984375
- w_conv_in: bfloat16 [1024, 2048], P('tp'), may hold values from -0.125 to 0.125
- w_conv_gate: bfloat16 [1024, 2048], P('tp'), may hold values from -0.125 to 0.125
- conv_kernel: bfloat16 [31, 1024], P(None, 'tp'), may hold values from -4.3105272 to 4.3105272
- ln_gain: bfloat16 [1024], P('tp'), may hold values from 0.099609375 to 1.8984375
- w_query: bfloat16 [1024, 2048], P('tp'), may hold values from -0.53033009 to 0.53033009
- w_key: bfloat16 [1024, 2048], P('tp'), may hold values from -0.53033009 to 0.53033009
- w_value: bfloat16 [1024, 2048], P('tp'), may hold values from -0.125 to 0.125
- cum_gate: float32 [16, 16384], P('tp', ('grp', 'sp')), parts along dimension 1, may hold values from -8192 to 0, as said below
- w_conv_out: bfloat16 [1024, 2048], P('tp'), may hold values from -0.125 to 0.125
- w_attn_out: bfloat16 [1024, 2048], P('tp'), may hold values from -0.125 to 0.125
Outputs:
- mixed: bfloat16 [16384, 2048], P(('grp', 'sp', 'tp')), parts along dimension 0
- log_total: float32 [16, 16384], P('tp', ('grp', 'sp')), parts along dimension 1
There are 2 independent parts, one for each index of `grp`. A program takes and returns all parts, laid end to end along the dimension named above; an argument that names none is the same for every part. Nothing has to cross between parts.
Inputs may be any that keep to these rules, and one draw needn't show every extreme that they name: cum_gate never rises along positions: entry t is the sum of the head's log forget gates at positions 0 to t.
All inputs are finite; a program needn't handle non-finite values.
Results may differ from a plain program's by a relative error of at most 0.0144.
Values may be sent and summed in bfloat16 or wider, within the bound.
A program may use at most 64 MiB of HBM per device.

v0:
```python
import jax
import jax.numpy as jnp
from jax import lax
from jax.sharding import PartitionSpec as P

D = 2048
CONV_CH = 1024


neg_large = -1e30


def sent_to_all(shard, axis):
    devices = lax.axis_size(axis)
    return lax.all_to_all(
        jnp.broadcast_to(shard[None], (devices, *shard.shape)), axis, 0, 0, tiled=True
    )


def in_order(parts, dim):
    lengths = list(parts.shape[1:])
    lengths[dim] *= parts.shape[0]
    return jnp.moveaxis(parts, 0, dim).reshape(lengths)


def gather_directly(shard, axis, dim):
    parts = sent_to_all(shard, axis)
    return in_order(parts, dim)


def passed_along(block, axis, distance):
    devices = range(lax.axis_size(axis))
    route = [(i - distance, i) for i in devices if i - distance in devices]
    return lax.ppermute(block, axis, route)


def sent_together(arrays, axis, dim, along):
    both = jnp.concatenate(arrays, axis=along)
    filled, at, outs = (lax.all_gather(both, axis, axis=dim, tiled=True), 0, [])
    for a in arrays:
        outs.append(lax.slice_in_dim(filled, at, at + a.shape[along], axis=along))
        at += a.shape[along]
    return tuple(outs)


def in_blocks(shard, dim, devices):
    lengths = shard.shape
    parts = shard.reshape(*lengths[:dim], devices, lengths[dim] // devices, *lengths[dim + 1 :])
    return jnp.moveaxis(parts, dim, 0)


def summed_on_arrival(shard, axis, dim):
    devices = lax.axis_size(axis)
    parts = lax.all_to_all(in_blocks(shard, dim, devices), axis, 0, 0, tiled=True)
    return jnp.sum(parts.astype(jnp.float32), axis=0)


def block_terms(q_blk, q_cum, k_blk, v_blk, k_cum, q_first, k_first):
    score_scale = q_blk.shape[2] ** (-0.5)
    scores = (
        jnp.einsum("qhd,khd->hqk", q_blk, k_blk, preferred_element_type=jnp.float32) * score_scale
    )
    scores = scores + q_cum[:, :, None] - k_cum[:, None, :]
    q_pos = q_first + jnp.arange(q_blk.shape[0], dtype=jnp.int32)
    k_pos = k_first + jnp.arange(k_blk.shape[0], dtype=jnp.int32)
    allowed = k_pos[None, :] <= q_pos[:, None]
    scores = jnp.where(allowed[None], scores, -jnp.inf)
    block_top = jnp.max(scores, axis=-1)
    weights = jnp.exp(scores - block_top[..., None])
    block_total = jnp.sum(weights, axis=-1)
    block_out = jnp.einsum(
        "hqk,khd->hqd", weights.astype(jnp.bfloat16), v_blk, preferred_element_type=jnp.float32
    ).astype(jnp.bfloat16)
    return (block_top, block_total, block_out)


def merge_terms(state, terms):
    top_now, total_now, acc_now = state
    block_top, block_total, block_out = terms
    top_new = jnp.maximum(top_now, block_top)
    keep_old = jnp.exp(top_now - top_new)
    keep_new = jnp.exp(block_top - top_new)
    return (
        top_new,
        total_now * keep_old + block_total * keep_new,
        acc_now * keep_old[..., None] + block_out.astype(jnp.float32) * keep_new[..., None],
    )


def local(
    inputs,
    norm_gain,
    w_conv_in,
    w_conv_gate,
    conv_kernel,
    ln_gain,
    w_query,
    w_key,
    w_value,
    cum_gate,
    w_conv_out,
    w_attn_out,
):
    rows_here = inputs.shape[0]
    conv_width = w_conv_in.shape[0]
    attn_width = w_query.shape[0]
    heads_here = cum_gate.shape[0]
    head_dim = attn_width // heads_here
    taps_count = conv_kernel.shape[0]
    w_all = jnp.concatenate([w_conv_in, w_conv_gate, w_query, w_key, w_value], axis=0)
    gain_all = norm_gain.astype(jnp.float32)
    contract_dims = (((1,), (1,)), ((), ()))
    piece_f = gather_directly(inputs, "tp", 1).astype(jnp.float32)
    scaled_piece = (piece_f * gain_all[None, :]).astype(jnp.bfloat16)
    raw_proj = lax.dot_general(
        scaled_piece, w_all, contract_dims, preferred_element_type=jnp.float32
    )
    squares = jnp.sum(piece_f * piece_f, axis=1)
    rms = lax.rsqrt(squares / D + 1e-06)[:, None]
    proj = raw_proj * rms
    conv_in = proj[:, :conv_width]
    conv_gate = proj[:, conv_width : 2 * conv_width]
    query = proj[:, 2 * conv_width : 2 * conv_width + attn_width].astype(jnp.bfloat16)
    key_rows = proj[:, 2 * conv_width + attn_width : 2 * conv_width + 2 * attn_width].astype(
        jnp.bfloat16
    )
    value = proj[:, 2 * conv_width + 2 * attn_width :].astype(jnp.bfloat16)
    glu = (conv_in * jax.nn.sigmoid(conv_gate)).astype(jnp.bfloat16)
    rim_rows = passed_along(glu[rows_here - (taps_count - 1) :], "sp", 1)
    extended = jnp.concatenate([rim_rows, glu], axis=0)
    kernel = conv_kernel.astype(jnp.float32)
    conv_sum = jnp.zeros((rows_here, conv_width), jnp.float32)
    for tap_idx in range(taps_count):
        conv_sum = (
            conv_sum
            + extended[tap_idx : tap_idx + rows_here].astype(jnp.float32) * kernel[tap_idx][None, :]
        )
    chan_first, chan_second = lax.psum(
        (jnp.sum(conv_sum, axis=1), jnp.sum(conv_sum * conv_sum, axis=1)), "tp"
    )
    chan_mean = (chan_first / CONV_CH)[:, None]
    chan_var = (chan_second / CONV_CH)[:, None] - chan_mean * chan_mean
    normed = (
        (conv_sum - chan_mean) * lax.rsqrt(chan_var + 1e-05) * ln_gain.astype(jnp.float32)[None, :]
    )
    conv_out = jax.nn.silu(normed).astype(jnp.bfloat16)
    q_heads = query.reshape(rows_here, heads_here, head_dim)
    cum_all = lax.all_gather(cum_gate.T, "sp", axis=0, tiled=True)
    own_first = lax.axis_index("sp") * rows_here
    start_state = (
        jnp.full((heads_here, rows_here), neg_large, jnp.float32),
        jnp.zeros((heads_here, rows_here), jnp.float32),
        jnp.zeros((heads_here, rows_here, head_dim), jnp.float32),
    )
    state = start_state
    k_piece, v_piece = sent_together((key_rows, value), "sp", 0, 1)
    block_count = k_piece.shape[0] // rows_here
    k_split = k_piece.reshape(block_count, rows_here, heads_here, head_dim)
    v_split = v_piece.reshape(block_count, rows_here, heads_here, head_dim)

    def visit(carry, item):
        k_blk, v_blk, block_idx = item
        k_first = block_idx * rows_here
        k_cum = lax.dynamic_slice_in_dim(cum_all, k_first, rows_here, 0).T

        def take_block(inner):
            return merge_terms(
                inner, block_terms(q_heads, cum_gate, k_blk, v_blk, k_cum, own_first, k_first)
            )

        def skip_block(inner):
            return inner

        return (lax.cond(k_first <= own_first, take_block, skip_block, carry), None)

    state, unused = lax.scan(
        visit, state, (k_split, v_split, jnp.arange(block_count, dtype=jnp.int32))
    )
    top_all, total_all, acc_all = state
    attn_out = (
        (acc_all / total_all[..., None])
        .transpose(1, 0, 2)
        .reshape(rows_here, attn_width)
        .astype(jnp.bfloat16)
    )
    log_total = top_all + jnp.log(total_all)
    mixed = summed_on_arrival(
        (
            jnp.dot(conv_out, w_conv_out, preferred_element_type=jnp.float32)
            + jnp.dot(attn_out, w_attn_out, preferred_element_type=jnp.float32)
        ).astype(jnp.bfloat16),
        "tp",
        0,
    ).astype(jnp.bfloat16)
    return (mixed, log_total)


def solution(mesh):
    in_specs = (
        P(("grp", "sp"), "tp"),
        P(),
        P("tp", None),
        P("tp", None),
        P(None, "tp"),
        P("tp"),
        P("tp", None),
        P("tp", None),
        P("tp", None),
        P("tp", ("grp", "sp")),
        P("tp", None),
        P("tp", None),
    )
    out_specs = (P(("grp", "sp", "tp"), None), P("tp", ("grp", "sp")))
    return jax.shard_map(local, mesh=mesh, in_specs=in_specs, out_specs=out_specs, check_vma=False)
```

profile of v0, /device:TPU:2016, one launch (start us, length us, event | category | flops | bytes accessed | tf_op | source)
XLA Modules:
  0.0 345.3 jit_solution(744768911133563822)
XLA Ops:
  9.4 4.6 %all-to-all-start = ((bf16[8,256,256]{1,2,0:T(8,128)(2,1)}), bf16[8,256,256]{1,2,0:T(8,128)(2,1)S(1)}, u32[]{:S(2)}, u32[]{:S(2)}) async-start(bf16[8,256,256]{1,2,0:T(8,128)(2,1)} %broadcast_in_dim.25), calls=%async_computation | async-start | bytes 2097152 | tf_op jit(solution)/shard_map/all_to_all | solution.py:15
  18.3 11.6 %all-to-all-done = bf16[8,256,256]{1,2,0:T(8,128)(2,1)S(1)} async-done(((bf16[8,256,256]{1,2,0:T(8,128)(2,1)}), bf16[8,256,256]{1,2,0:T(8,128)(2,1)S(1)}, u32[]{:S(2)}, u32[]{:S(2)}) %all-to-all-start) | async-done | bytes 1048608 | tf_op jit(solution)/shard_map/all_to_all | solution.py:15
  30.6 2.8 fusion.62
  35.6 53.0 %all_gather.6 = f32[8192,2]{0,1:T(2,128)S(1)} all-gather(f32[256,2]{0,1:T(2,128)S(1)} %bitcast.102), channel_id=1, replica_groups=mesh['grp'=2,'sp'=32,'tp'=8] {'sp'}, dimensions={0}, use_global_device_ids=true | all-gather | bytes 67584 | tf_op jit(solution)/shard_map/all_gather | solution.py:148
  89.5 12.5 %all-reduce = (f32[256]{0:T(256)S(1)}, f32[256]{0:T(256)S(1)}) all-reduce(f32[256]{0:T(256)S(1)} %get-tuple-element.184, f32[256]{0:T(256)S(1)} %get-tuple-element.183), channel_id=1, replica_groups=mesh['grp'=2,'sp'=32,'tp'=8] {'tp'}, use_global_device_ids=true, to_apply=%region_4.0 | all-reduce | flops 512 | bytes 4096 | tf_op jit(solution)/shard_map/psum | solution.py:138
  102.5 53.7 %all-gather.2.cloned.1.call-done = bf16[8192,256]{1,0:T(8,128)(2,1)} async-done(((bf16[256,256]{1,0:T(8,128)(2,1)}), bf16[8192,256]{1,0:T(8,128)(2,1)}) %all-gather.2.cloned.1.call-update) | async-done | bytes 4194320 | tf_op jit(solution)/shard_map/all_gather | solution.py:39
  156.1 4.5 %fusion.61 = (bf16[8192,128]{1,0:T(8,128)(2,1)}, bf16[8192,128]{1,0:T(8,128)(2,1)}) fusion(bf16[8192,256]{1,0:T(8,128)(2,1)} %all-gather.2.cloned.1.call-done), kind=kLoop, calls=%fused_computation.157 | loop fusion | bytes 8388608 | tf_op jit(solution)/shard_map/slice | solution.py:41
  160.6 8.2 %reshape.86 = bf16[32,256,2,64]{3,2,1,0:T(2,128)(2,1)} reshape(bf16[8192,128]{1,0:T(8,128)(2,1)} %get-tuple-element.218) | data formatting | bytes 4194304 | tf_op jit(solution)/shard_map/reshape | solution.py:159
  168.8 9.7 %copy.24 = bf16[32,256,2,64]{1,3,2,0:T(8,128)(2,1)} copy(bf16[32,256,2,64]{3,2,1,0:T(2,128)(2,1)} %reshape.86) | data formatting | bytes 4194304 | tf_op jit(solution)/shard_map/while | solution.py:176
  178.5 8.2 %reshape.85 = bf16[32,256,2,64]{3,2,1,0:T(2,128)(2,1)} reshape(bf16[8192,128]{1,0:T(8,128)(2,1)} %get-tuple-element.219) | data formatting | bytes 4194304 | tf_op jit(solution)/shard_map/reshape | solution.py:158
  186.7 9.8 %copy.23 = bf16[32,256,2,64]{1,3,2,0:T(8,128)(2,1)} copy(bf16[32,256,2,64]{3,2,1,0:T(2,128)(2,1)} %reshape.85) | data formatting | bytes 4194304 | tf_op jit(solution)/shard_map/while | solution.py:176
  196.5 119.1 %while.14 = (s32[]{:T(128)}, f32[2,256]{1,0:T(2,128)S(1)}, f32[2,256]{1,0:T(2,128)S(1)}, f32[2,256,64]{1,2,0:T(8,128)S(1)}, s32[32]{0:T(128)S(1)}, /*index=5*/s3...) while((s32[]{:T(128)}, f32[2,256]{1,0:T(2,128)S(1)}, ...), condition=%wide.region_10.11_spmd, body=%wide.region_5.10_spmd.sunk | while | flops 34966024 | bytes 2205049 | solution.py:176
  197.7 2.5 conditional.2
  201.4 2.5 conditional.2
  205.2 2.5 conditional.2
  212.6 2.5 conditional.2
  216.3 2.5 conditional.2
  227.5 2.5 conditional.2
  231.2 2.5 conditional.2
  242.4 2.5 conditional.2
  246.1 2.5 conditional.2
  257.3 2.5 conditional.2
  261.0 2.5 conditional.2
  272.2 2.5 conditional.2
  275.9 2.5 conditional.2
  283.3 2.5 conditional.2
  287.1 2.5 conditional.2
  298.2 2.5 conditional.2
  301.9 2.5 conditional.2
  313.1 2.5 conditional.2
  317.1 4.5 %all-to-all-start.1 = ((bf16[8,32,2048]{2,1,0:T(8,128)(2,1)}), bf16[8,32,2048]{2,1,0:T(8,128)(2,1)S(1)}, u32[]{:S(2)}, u32[]{:S(2)}) async-start(bf16[8,32,2048]{2,1,0:T(8,128)(2,1)} %bitcast.99), calls=%async_computation.1 | async-start | bytes 2097152 | tf_op jit(solution)/shard_map/all_to_all | solution.py:54
  322.3 15.3 %all-to-all-done.1 = bf16[8,32,2048]{2,1,0:T(8,128)(2,1)S(1)} async-done(((bf16[8,32,2048]{2,1,0:T(8,128)(2,1)}), bf16[8,32,2048]{2,1,0:T(8,128)(2,1)S(1)}, u32[]{:S(2)}, u32[]{:S(2)}) %all-to-all-start.1) | async-done | bytes 1048608 | tf_op jit(solution)/shard_map/all_to_all | solution.py:54
  (327 shorter events, 146.7 us)
Async XLA Ops:
  7.2 94.8 %copy-start = (bf16[128,2048]{1,0:T(8,128)(2,1)S(1)}, bf16[128,2048]{1,0:T(8,128)(2,1)}, u32[]{:S(2)}) copy-start(bf16[128,2048]{1,0:T(8,128)(2,1)} %param.26) | copy-start | bytes 1572868
  7.2 6.9 %copy-start.8 = (bf16[2048]{0:T(1024)(128)(2,1)S(1)}, bf16[2048]{0:T(1024)(128)(2,1)}, u32[]{:S(2)}) copy-start(bf16[2048]{0:T(1024)(128)(2,1)} %param.17) | copy-start | bytes 12292
  7.2 6.9 %copy-start.2 = (bf16[128,2048]{1,0:T(8,128)(2,1)S(1)}, bf16[128,2048]{1,0:T(8,128)(2,1)}, u32[]{:S(2)}) copy-start(bf16[128,2048]{1,0:T(8,128)(2,1)} %param.18) | copy-start | bytes 1572868
  7.2 7.7 %copy-start.3 = (bf16[128,2048]{1,0:T(8,128)(2,1)S(1)}, bf16[128,2048]{1,0:T(8,128)(2,1)}, u32[]{:S(2)}) copy-start(bf16[128,2048]{1,0:T(8,128)(2,1)} %param.19) | copy-start | bytes 1572868
  8.3 7.5 %copy-start.4 = (bf16[128,2048]{1,0:T(8,128)(2,1)S(1)}, bf16[128,2048]{1,0:T(8,128)(2,1)}, u32[]{:S(2)}) copy-start(bf16[128,2048]{1,0:T(8,128)(2,1)} %param.22) | copy-start | bytes 1572868
  9.4 20.5 %all-to-all-start = ((bf16[8,256,256]{1,2,0:T(8,128)(2,1)}), bf16[8,256,256]{1,2,0:T(8,128)(2,1)S(1)}, u32[]{:S(2)}, u32[]{:S(2)}) async-start(bf16[8,256,256]{1,2,0:T(8,128)(2,1)} %broadcast_in_dim.25), calls=%async_computation | async-start | bytes 2097152 | tf_op jit(solution)/shard_map/all_to_all | solution.py:15
  14.0 142.1 %all-gather.2.cloned.1.call-start = ((), (), s32[]{:S(2)}) async-start(), calls=%async_computation.2 | async-start | bytes 4325376 | tf_op jit(solution)/shard_map/all_gather | solution.py:39
  14.1 2.6 copy-start.5
  14.1 3.4 copy-start.6
  30.6 3.6 %copy-start.7 = (bf16[31,128]{1,0:T(8,128)(2,1)S(1)}, bf16[31,128]{1,0:T(8,128)(2,1)}, u32[]{:S(2)}) copy-start(bf16[31,128]{1,0:T(8,128)(2,1)} %param.20) | copy-start | bytes 23812
  30.6 5.0 %copy-start.9 = (f32[2,256]{1,0:T(2,128)S(1)}, f32[2,256]{1,0:T(2,128)}, u32[]{:S(2)}) copy-start(f32[2,256]{1,0:T(2,128)} %param.25) | copy-start | bytes 6148
  30.6 58.0 %copy-start.10 = (bf16[128]{0:T(256)(128)(2,1)S(1)}, bf16[128]{0:T(256)(128)(2,1)}, u32[]{:S(2)}) copy-start(bf16[128]{0:T(256)(128)(2,1)} %param.21) | copy-start | bytes 772
  34.3 54.5 %collective-permute-start = (bf16[30,128]{1,0:T(8,128)(2,1)S(1)}, bf16[30,128]{1,0:T(8,128)(2,1)S(1)}, u32[]{:S(2)}, u32[]{:S(2)}) collective-permute-start(bf16[30,128]{1,0:T(8,128)(2,1)S(1)} %slice.282), channel_id=1, source_target_pairs={{0,8},{8,16},{16,24},{24,32},{32,40},{40,48},{48,56},{56,64},{64,7... | collective-permute-start | bytes 23048 | tf_op jit(solution)/shard_map/ppermute | solution.py:34
  196.5 119.2 %copy-start.1 = (bf16[128,2048]{1,0:T(8,128)(2,1)S(1)}, bf16[128,2048]{1,0:T(8,128)(2,1)}, u32[]{:S(2)}) copy-start(bf16[128,2048]{1,0:T(8,128)(2,1)} %param.27) | copy-start | bytes 1572868
  317.1 20.5 %all-to-all-start.1 = ((bf16[8,32,2048]{2,1,0:T(8,128)(2,1)}), bf16[8,32,2048]{2,1,0:T(8,128)(2,1)S(1)}, u32[]{:S(2)}, u32[]{:S(2)}) async-start(bf16[8,32,2048]{2,1,0:T(8,128)(2,1)} %bitcast.99), calls=%async_computation.1 | async-start | bytes 2097152 | tf_op jit(solution)/shard_map/all_to_all | solution.py:54
Sparse Core Ops, SparseCore 0:
  34.3 121.7 all-gather.1
where the time goes:
time: 349 us; the launch traced here: 345 us
  waiting for transfers between devices  80.7 us (23%)
  matrix products  76.5 us (22%)
  local copies, waits for them, and re-layouts  66.7 us (19%)
  blocking collectives  65.5 us (19%)
  loops' own time  21.1 us (6%)
  between operations  14.3 us (4%)
  starting transfers between devices  10.5 us (3%)
  other arithmetic  10 us (3%)
    all_gather x1, waiting for transfers between devices, sent_together(): filled, at, outs = (lax.all_gather(both, axis, axis=dim, tiled=True), 0, [])  53.7 us
    all_gather x1, blocking collectives, local(): cum_all = lax.all_gather(cum_gate.T, 'sp', axis=0, tiled=True)  53 us
    dot_general x32, matrix products, block_terms(): jnp.einsum('qhd,khd->hqk', q_blk, k_blk, preferred_element_type=jnp.float32)  37.2 us
    dot_general x32, matrix products, block_terms(): jnp.einsum('hqk,khd->hqd', weights.astype(jnp.bfloat16), v_blk, preferred...  34.5 us
    another operation x1, loops' own time, local(): lax.scan(visit, state, (k_split, v_split, jnp.arange(block_count, dtype=j...  19.5 us
    while x2, local copies, waits for them, and re-layouts, local(): lax.scan(visit, state, (k_split, v_split, jnp.arange(block_count, dtype=j...  19.5 us
    dynamic_slice x32, local copies, waits for them, and re-layouts, local(): lax.scan(visit, state, (k_split, v_split, jnp.arange(block_count, dtype=j...  18.8 us
    all_to_all x1, waiting for transfers between devices, summed_on_arrival(): lax.all_to_all(in_blocks(shard, dim, devices), axis, 0, 0, tiled=True)  15.3 us
  transfers between devices with their start and end apart: 4, of which 3 were waited for; matrix products, arithmetic and copies ran while one was open for 2% of the time, Pallas kernels for 0%

commit v1 on v0

v1 whole, which is shorter than its diff:
```python
import functools

import jax
import jax.numpy as jnp
from jax import lax
from jax.experimental import pallas as pl
from jax.experimental.pallas import tpu as pltpu
from jax.sharding import PartitionSpec as P

MESH = pl.DeviceIdType.MESH
F32 = jnp.float32
BF16 = jnp.bfloat16
CHUNKS = 4
OUT_CUTS = 2
NT = (((1,), (1,)), ((), ()))
NN = (((1,), (0,)), ((), ()))


def dot(a, b, dims):
    return lax.dot_general(a, b, dims, preferred_element_type=F32)


def layer(
    n,
    n_tp,
    x_hbm,
    gain_hbm,
    wci_hbm,
    wcg_hbm,
    taps_hbm,
    lng_hbm,
    wq_hbm,
    wk_hbm,
    wv_hbm,
    cum_hbm,
    wco_hbm,
    wao_hbm,
    mixed_ref,
    log_ref,
    xg,
    xs,
    gain,
    taps,
    lng,
    wkv,
    w3,
    wo,
    kv,
    cum,
    kvacc,
    sq,
    qs,
    m_ref,
    l_ref,
    acc,
    ext,
    glu_tail,
    halo,
    ctr,
    stats,
    comb,
    pair_out,
    pair_in,
    xout,
    xin,
    ld_sem,
    in_send,
    in_recv,
    kv_send,
    kv_recv,
    cum_send,
    cum_recv,
    halo_sem,
    st_send,
    st_recv,
    pair_send,
    pair_recv,
    x_send,
    x_recv,
):
    z = lax.axis_index("sp")
    t = lax.axis_index("tp")
    rows, feat = x_hbm.shape
    width = wk_hbm.shape[0]
    heads = cum_hbm.shape[0]
    hd = width // heads
    n_taps = taps_hbm.shape[0]
    half_n = n // 2
    nx = n_tp // 2
    x = t // 2
    c = t % 2

    def at(dx, core):
        return 2 * ((x + dx + nx) % nx) + core

    right, left, far, mate = at(1, c), at(-1, c), at(2, c), at(0, 1 - c)
    up, down = (z + 1) % n, (z + n - 1) % n

    def rdma(src, dst, send, recv, **device):
        return pltpu.make_async_remote_copy(
            src_ref=src, dst_ref=dst, send_sem=send, recv_sem=recv, device_id=device, device_id_type=MESH
        )

    loads = [
        (x_hbm, xg.at[t]),
        (wk_hbm, wkv.at[pl.ds(0, width)]),
        (wv_hbm, wkv.at[pl.ds(width, width)]),
        (gain_hbm, gain),
        (cum_hbm, cum.at[z]),
        (wci_hbm, w3.at[pl.ds(0, width)]),
        (wcg_hbm, w3.at[pl.ds(width, width)]),
        (wq_hbm, w3.at[pl.ds(2 * width, width)]),
        (taps_hbm, taps),
        (lng_hbm, lng),
        (wco_hbm, wo.at[pl.ds(0, width)]),
        (wao_hbm, wo.at[pl.ds(width, width)]),
    ]
    loads = [pltpu.make_async_copy(a, b, ld_sem.at[i]) for i, (a, b) in enumerate(loads)]
    for copy in loads:
        copy.start()

    barrier = pltpu.get_barrier_semaphore()
    for k in range(1, n_tp):
        pl.semaphore_signal(barrier, inc=1, device_id={"tp": (t + k) % n_tp}, device_id_type=MESH)
    pl.semaphore_signal(barrier, inc=1, device_id={"sp": up}, device_id_type=MESH)
    pl.semaphore_signal(barrier, inc=1, device_id={"sp": down}, device_id_type=MESH)
    pl.semaphore_wait(barrier, n_tp + 1)

    half = rows // 2
    pending = []

    def part(slot, h):
        return xg.at[slot, pl.ds(h * half, half)]

    def send_in(slot, h, to):
        k = len(pending)
        copy = rdma(part(slot, h), part(slot, h), in_send.at[k], in_recv.at[slot, h], tp=to)
        copy.start()
        pending.append(copy)

    def got(slot, h):
        rdma(part(slot, h), part(slot, h), in_send.at[0], in_recv.at[slot, h], tp=mate).wait_recv()

    loads[0].wait()
    send_in(t, 0, right)
    send_in(t, 1, left)
    send_in(t, 1, right)
    send_in(t, 0, left)
    send_in(t, 0, mate)
    send_in(t, 1, mate)
    for copy in loads[1:4]:
        copy.wait()
    kvacc[...] = jnp.zeros_like(kvacc)
    sq[...] = jnp.zeros_like(sq)

    def process(slot):
        xf = xg[slot].astype(F32)
        lanes = pl.ds(pl.multiple_of(slot * feat, feat), feat)
        s2 = xf * xf
        sq[...] += s2[:, :128] + s2[:, 128:]
        sc = (xf * gain[:, lanes].astype(F32)).astype(BF16)
        xs[slot] = sc
        kvacc[...] += dot(sc, wkv[:, lanes], NT)

    process(t)
    got(mate, 0)
    got(mate, 1)
    process(mate)
    got(left, 0)
    send_in(left, 0, right)
    send_in(left, 0, mate)
    got(right, 1)
    send_in(right, 1, left)
    send_in(right, 1, mate)
    got(left, 1)
    send_in(left, 1, mate)
    got(right, 0)
    send_in(right, 0, mate)
    process(left)
    process(right)
    for slot in (at(-1, 1 - c), at(1, 1 - c)):
        got(slot, 0)
        got(slot, 1)
        process(slot)
    got(far, 0)
    send_in(far, 0, mate)
    got(far, 1)
    send_in(far, 1, mate)
    process(far)
    got(at(2, 1 - c), 0)
    got(at(2, 1 - c), 1)
    process(at(2, 1 - c))

    rms = lax.rsqrt(jnp.sum(sq[...], axis=1, keepdims=True) / (feat * n_tp) + 1e-06)
    kv[z] = (kvacc[...] * rms).astype(BF16)
    loads[4].wait()

    chunk = rows // CHUNKS

    def kv_copy(way, blk, q, k, to):
        ref = kv.at[blk, pl.ds(q * chunk, chunk)]
        return rdma(ref, ref, kv_send.at[way, k, q], kv_recv.at[blk, q], sp=to)

    def cum_copy(way, blk, k, to):
        return rdma(cum.at[blk], cum.at[blk], cum_send.at[way, k], cum_recv.at[blk], sp=to)

    first_up = z < n - 1
    first_down = z <= half_n - 2
    for way, cond, to in ((0, first_up, up), (1, first_down, down)):

        @pl.when(cond)
        def _(way=way, to=to):
            cum_copy(way, z, 0, to).start()
            for q in range(CHUNKS):
                kv_copy(way, z, q, 0, to).start()

    for copy in loads[5:8]:
        copy.wait()
    r3 = dot(xs[0], w3[:, :feat], NT)
    for p in range(1, n_tp):
        r3 += dot(xs[p], w3[:, p * feat : (p + 1) * feat], NT)
    r3 = r3 * rms
    glu = (r3[:, :width] * jax.nn.sigmoid(r3[:, width : 2 * width])).astype(BF16)
    pad = glu_tail.shape[0]
    glu_tail[...] = glu[rows - pad :]
    ext[pl.ds(pad, rows)] = glu.astype(F32)
    ext[pl.ds(pad + rows, 8)] = jnp.zeros((8, width), F32)
    query = (r3[:, 2 * width :]).astype(BF16) * jnp.asarray(hd ** (-0.5), BF16)
    lane = lax.broadcasted_iota(jnp.int32, (rows, width), 1)
    for h in range(heads):
        mine = (lane >= h * hd) & (lane < (h + 1) * hd)
        qs[pl.ds(h * rows, rows)] = jnp.where(mine, query.astype(F32), 0.0).astype(BF16)
    m_ref[...] = jnp.full_like(m_ref, -1e30)
    l_ref[...] = jnp.zeros_like(l_ref)
    acc[...] = jnp.zeros_like(acc)
    halo_copy = rdma(glu_tail, halo, halo_sem.at[0], halo_sem.at[1], sp=up)

    @pl.when(first_up)
    def _():
        halo_copy.start()

    piece = heads * rows // CHUNKS
    per_head = rows // piece

    def attend(q, blk, offset):
        h = q // per_head
        here = pl.ds(q * piece, piece)
        s = dot(qs[here], kv[blk, :, :width], NT)
        s = s + (cum[z, h : h + 1, 0:1] - cum[blk, h : h + 1, :])
        q_pos = lax.broadcasted_iota(jnp.int32, s.shape, 0) + (q % per_head) * piece + offset
        k_pos = lax.broadcasted_iota(jnp.int32, s.shape, 1)
        s = jnp.where(k_pos <= q_pos, s, -1e30)
        m_old = m_ref[here]
        m_new = jnp.maximum(m_old, jnp.max(s, axis=1, keepdims=True))
        fade = jnp.exp(m_old - m_new)
        p = jnp.exp(s - m_new[:, :1])
        l_ref[here] = l_ref[here] * fade + jnp.sum(p, axis=1, keepdims=True)
        m_ref[here] = m_new
        acc[here] = acc[here] * fade + dot(p.astype(BF16), kv[blk, :, width:], NN)

    def convolve():
        loads[8].wait()

        @pl.when(z > 0)
        def _():
            halo_copy.wait_recv()
            ext[pl.ds(0, pad)] = halo[...].astype(F32)

        @pl.when(z == 0)
        def _():
            ext[pl.ds(0, pad)] = jnp.zeros((pad, width), F32)

        weight = taps[...].astype(F32)
        shift = pad - (n_taps - 1)
        long = rows + 8
        total = jnp.zeros((rows, width), F32)
        for r in range(8):
            sub = None
            for j in range(n_taps):
                if (shift + j) % 8 == r:
                    base = shift + j - r
                    if r == 0:
                        term = ext[pl.ds(base, rows)] * weight[j : j + 1]
                    else:
                        term = ext[pl.ds(base, long)] * weight[j : j + 1]
                    sub = term if sub is None else sub + term
            if r == 0:
                total = total + sub
            else:
                total = total + pltpu.roll(sub, long - r, 0)[:rows]
        turned = total.T
        ctr[...] = turned
        stats[t, 0:1] = jnp.sum(turned, axis=0, keepdims=True)
        stats[t, 1:2] = jnp.sum(turned * turned, axis=0, keepdims=True)

    def stat_copy(k):
        return rdma(stats.at[t], stats.at[t], st_send.at[k], st_recv.at[t], tp=(t + k) % n_tp)

    def send_stats():
        for k in range(1, n_tp):
            stat_copy(k).start()

    def finish_conv():
        for k in range(1, n_tp):
            src = (t + k) % n_tp
            rdma(stats.at[src], stats.at[src], st_send.at[0], st_recv.at[src], tp=src).wait_recv()
        loads[9].wait()
        tot = stats[0]
        for p in range(1, n_tp):
            tot = tot + stats[p]
        mean = tot[0:1] / (width * n_tp)
        var = tot[1:2] / (width * n_tp) - mean * mean
        y = ((ctr[...] - mean) * lax.rsqrt(var + 1e-05)).T
        y = y * lng[...].astype(F32)
        y = (y * jax.nn.sigmoid(y)).astype(BF16)
        each = rows // n_tp
        for d in range(n_tp):
            comb[d // 2, d % 2, :, :width] = y[d * each : (d + 1) * each]

    conv_at = 2
    stats_at = min(5, half_n + 1)

    def flows(s):
        cw_in = (z >= s) & (s <= half_n)
        cw_on = cw_in & (z < n - 1) & (s < half_n)
        reach = (z + s <= half_n - 2) | (z + s >= n)
        cc_in = reach & (s <= half_n - 1)
        cc_on = cc_in & (s < half_n - 1)
        return cw_in, cw_on, cc_in, cc_on

    def step(s, carry):
        cw_in, cw_on, cc_in, cc_on = flows(s)
        j_cw, j_cc = (z + n - s) % n, (z + s) % n
        b_cw, b_cc = (z + n - s + 1) % n, (z + s - 1) % n
        use_cw = z >= s - 1
        use_cc = (z + s - 1 >= n) & (s <= half_n)
        for q in range(CHUNKS):
            for way, arrives, goes, blk, to in (
                (0, cw_in, cw_on, j_cw, up),
                (1, cc_in, cc_on, j_cc, down),
            ):

                @pl.when(arrives)
                def _(way=way, blk=blk, to=to):
                    if q == 0:
                        cum_copy(way, blk, 0, to).wait_recv()
                    kv_copy(way, blk, q, 0, to).wait_recv()

                @pl.when(goes)
                def _(way=way, blk=blk, to=to):
                    if q == 0:
                        cum_copy(way, blk, s, to).start()
                    kv_copy(way, blk, q, s, to).start()

            @pl.when(use_cw)
            def _():
                attend(q, b_cw, (s - 1) * rows)

            @pl.when(use_cc)
            def _():
                attend(q, b_cc, n * rows)

        @pl.when(s == conv_at)
        def _():
            convolve()
            send_stats()

        @pl.when(s == stats_at)
        def _():
            finish_conv()

        return carry

    lax.fori_loop(1, half_n + 2, step, 0)

    tops, sums = m_ref[...], l_ref[...]
    logs = tops + jnp.log(sums)
    attn = acc[...] / sums
    log_row = logs[:rows]
    attn_row = attn[:rows]
    for h in range(1, heads):
        attn_row = jnp.where(lane >= h * hd, attn[h * rows : (h + 1) * rows], attn_row)
        log_row = jnp.where(lane >= h, logs[h * rows : (h + 1) * rows], log_row)
    each = rows // n_tp
    attn_row = attn_row.astype(BF16)
    for d in range(n_tp):
        comb[d // 2, d % 2, :, width:] = attn_row[d * each : (d + 1) * each]

    for copy in loads[10:12]:
        copy.wait()
    cut = wo.shape[1] // OUT_CUTS

    def product(core, i):
        lhs = comb[:, core].reshape(nx * each, 2 * width)
        return dot(lhs, wo[:, i * cut : (i + 1) * cut], NN).reshape(nx, each, cut)

    pairs = []
    for i in range(OUT_CUTS):
        pair_out[i] = product(1 - c, i).astype(BF16)
        copy = rdma(pair_out.at[i], pair_in.at[i], pair_send.at[i], pair_recv.at[i], tp=mate)
        copy.start()
        pairs.append(copy)
    outs = []
    for i in range(OUT_CUTS):
        own = product(c, i)
        pairs[i].wait_recv()
        xout[i] = (own + pair_in[i].astype(F32)).astype(BF16)
        for dx in (2, 1, 3):
            dst = at(dx - nx, c)
            copy = rdma(
                xout.at[i, (x + dx) % nx], xin.at[i, dx - 1], x_send.at[i, dx - 1], x_recv.at[i, dx - 1], tp=dst
            )
            copy.start()
            outs.append((i, copy))
    log_ref[...] = log_row.T[:heads] + (cum[z] - cum[z][:, 0:1])
    for i in range(OUT_CUTS):
        total = xout[i, x].astype(F32)
        for k, copy in outs:
            if k == i:
                copy.wait_recv()
        for dx in range(nx - 1):
            total = total + xin[i, dx].astype(F32)
        mixed_ref[:, i * cut : (i + 1) * cut] = total.astype(BF16)

    for copy in pending:
        copy.wait_send()
    for way, cond, to in ((0, first_up, up), (1, first_down, down)):

        @pl.when(cond)
        def _(way=way, to=to):
            cum_copy(way, z, 0, to).wait_send()
            for q in range(CHUNKS):
                kv_copy(way, z, q, 0, to).wait_send()

    @pl.when(first_up)
    def _():
        halo_copy.wait_send()

    for k in range(1, n_tp):
        stat_copy(k).wait_send()

    def drain(s, carry):
        cw_in, cw_on, cc_in, cc_on = flows(s)
        for way, goes, blk, to in ((0, cw_on, (z + n - s) % n, up), (1, cc_on, (z + s) % n, down)):

            @pl.when(goes)
            def _(way=way, blk=blk, to=to):
                cum_copy(way, blk, s, to).wait_send()
                for q in range(CHUNKS):
                    kv_copy(way, blk, q, s, to).wait_send()

        return carry

    lax.fori_loop(1, half_n, drain, 0)
    for copy in pairs:
        copy.wait_send()
    for k, copy in outs:
        copy.wait_send()


def solution(mesh):
    n, n_tp = mesh.shape["sp"], mesh.shape["tp"]

    def local(
        inputs,
        norm_gain,
        w_conv_in,
        w_conv_gate,
        conv_kernel,
        ln_gain,
        w_query,
        w_key,
        w_value,
        cum_gate,
        w_conv_out,
        w_attn_out,
    ):
        rows, feat = inputs.shape
        width, full = w_key.shape
        heads = cum_gate.shape[0]
        n_taps = conv_kernel.shape[0]
        each = rows // n_tp
        nx = n_tp // 2
        pad = 32
        cut = full // OUT_CUTS
        half_n = n // 2
        dma = pltpu.SemaphoreType.DMA
        vmem = pltpu.VMEM
        scratch = [
            vmem((n_tp, rows, feat), BF16),
            vmem((n_tp, rows, feat), BF16),
            vmem((1, full), BF16),
            vmem((n_taps, width), BF16),
            vmem((1, width), BF16),
            vmem((2 * width, full), BF16),
            vmem((3 * width, full), BF16),
            vmem((2 * width, full), BF16),
            vmem((n, rows, 2 * width), BF16),
            vmem((n, heads, rows), F32),
            vmem((rows, 2 * width), F32),
            vmem((rows, 128), F32),
            vmem((heads * rows, width), BF16),
            vmem((heads * rows, width), F32),
            vmem((heads * rows, width), F32),
            vmem((heads * rows, width), F32),
            vmem((pad + rows + 8, width), F32),
            vmem((pad, width), BF16),
            vmem((pad, width), BF16),
            vmem((width, rows), F32),
            vmem((n_tp, 2, rows), F32),
            vmem((nx, 2, each, 2 * width), BF16),
            vmem((OUT_CUTS, nx, each, cut), BF16),
            vmem((OUT_CUTS, nx, each, cut), BF16),
            vmem((OUT_CUTS, nx, each, cut), BF16),
            vmem((OUT_CUTS, nx - 1, each, cut), BF16),
            dma((12,)),
            dma((14,)),
            dma((n_tp, 2)),
            dma((2, half_n, CHUNKS)),
            dma((n, CHUNKS)),
            dma((2, half_n)),
            dma((n,)),
            dma((2,)),
            dma((n_tp,)),
            dma((n_tp,)),
            dma((OUT_CUTS,)),
            dma((OUT_CUTS,)),
            dma((OUT_CUTS, nx - 1)),
            dma((OUT_CUTS, nx - 1)),
        ]
        return pl.pallas_call(
            functools.partial(layer, n, n_tp),
            out_shape=(
                jax.ShapeDtypeStruct((each, full), BF16),
                jax.ShapeDtypeStruct((heads, rows), F32),
            ),
            in_specs=[pl.BlockSpec(memory_space=pl.ANY)] * 12,
            out_specs=(pl.BlockSpec(memory_space=pltpu.VMEM), pl.BlockSpec(memory_space=pltpu.VMEM)),
            scratch_shapes=scratch,
            compiler_params=pltpu.CompilerParams(collective_id=0, has_side_effects=True),
        )(
            inputs,
            norm_gain.reshape(1, full),
            w_conv_in,
            w_conv_gate,
            conv_kernel,
            ln_gain.reshape(1, width),
            w_query,
            w_key,
            w_value,
            cum_gate,
            w_conv_out,
            w_attn_out,
        )

    in_specs = (
        P(("grp", "sp"), "tp"),
        P(),
        P("tp", None),
        P("tp", None),
        P(None, "tp"),
        P("tp"),
        P("tp", None),
        P("tp", None),
        P("tp", None),
        P("tp", ("grp", "sp")),
        P("tp", None),
        P("tp", None),
    )
    out_specs = (P(("grp", "sp", "tp"), None), P("tp", ("grp", "sp")))
    return jax.shard_map(local, mesh=mesh, in_specs=in_specs, out_specs=out_specs, check_vma=False)
```

time: 349 us -> 117 us (0.34)
  the two profiles are of different devices: /device:TPU:2016 before, /device:TPU:33 now
where the time goes in v1:
time: 117 us
  Pallas kernels  113 us (97%)
  local copies, waits for them, and re-layouts  3.44 us (3%)
    pallas_call x1, Pallas kernels, local(): pl.pallas_call(functools.partial(layer, n, n_tp), out_shape=(jax.ShapeDty...  113 us

profile of v1, /device:TPU:33, one launch (start us, length us, event | category | flops | bytes accessed | tf_op | source)
XLA Modules:
  0.0 117.1 jit_solution(17427197923818373881)
XLA Ops:
  0.6 1.3 %reshape.10.gain_hbm = bf16[1,2048]{1,0:T(2,128)(2,1)} reshape(bf16[2048]{0:T(1024)(128)(2,1)} %param.13) | data formatting | bytes 8192 | tf_op jit(solution)/shard_map/reshape | solution.py:543
  1.9 113.1 %shard_map.131 = (bf16[32,2048]{1,0:T(8,128)(2,1)}, f32[2,256]{1,0:T(2,128)}) custom-call(bf16[256,256]{1,0:T(8,128)(2,1)} %x_hbm.1, bf16[1,2048]{1,0:T(2,128)(2,1)} %reshape.10.gain_hbm, bf16[128,2048]{1,0:T(8,128)(2,1)} %wci_hbm.1, bf16[128,2048]{1,0:T(8,128)(2,1)} %wcg_hbm.1, bf16[31,128]{1,0:T(8,128)(2,1)} %taps_hbm.1, bf16[1,128]{1,0:T(2,128)(2,1)} %bitcast.1, ...), custom_call_target="tpu_custom_call" | custom-call | tf_op jit(solution)/shard_map/pallas_call | solution.py:531
  115.0 0.0 copy-start
  115.0 1.6 %copy.16 = bf16[32,2048]{1,0:T(8,128)(2,1)} copy(bf16[32,2048]{1,0:T(8,128)(2,1)} %get-tuple-element.4) | data formatting | bytes 262144
  116.6 0.0 copy-done
  116.6 0.6 copy.17
Async XLA Ops:
  115.0 1.6 %copy-start = (f32[2,256]{1,0:T(2,128)S(1)}, f32[2,256]{1,0:T(2,128)}, u32[]{:S(2)}) copy-start(f32[2,256]{1,0:T(2,128)} %get-tuple-element.5) | copy-start | bytes 6148

commit v2 on v1

--- a/solution.py
+++ b/solution.py
@@ -71,6 +71,8 @@
     cum_send,
     cum_recv,
     halo_sem,
+    up_ready,
+    far_ready,
     st_send,
     st_recv,
     pair_send,
@@ -122,9 +124,34 @@
     barrier = pltpu.get_barrier_semaphore()
     for k in range(1, n_tp):
         pl.semaphore_signal(barrier, inc=1, device_id={"tp": (t + k) % n_tp}, device_id_type=MESH)
-    pl.semaphore_signal(barrier, inc=1, device_id={"sp": up}, device_id_type=MESH)
-    pl.semaphore_signal(barrier, inc=1, device_id={"sp": down}, device_id_type=MESH)
-    pl.semaphore_wait(barrier, n_tp + 1)
+    last = n - 1
+    n_low = half_n - 1
+    is_low = z < n_low
+
+    @pl.when(z < last)
+    def _():
+        pl.semaphore_signal(barrier, inc=1, device_id={"sp": up}, device_id_type=MESH)
+
+    @pl.when(is_low)
+    def _():
+        pl.semaphore_signal(barrier, inc=1, device_id={"sp": last}, device_id_type=MESH)
+
+    pl.semaphore_wait(
+        barrier, n_tp - 1 + jnp.where(z > 0, 1, 0) + jnp.where(z == last, n_low, 0)
+    )
+
+    @pl.when(z > 0)
+    def _():
+        pl.semaphore_signal(up_ready, inc=1, device_id={"sp": down}, device_id_type=MESH)
+
+    @pl.when(z == last)
+    def _():
+        def tell(j, carry):
+            pl.semaphore_signal(far_ready, inc=1, device_id={"sp": j}, device_id_type=MESH)
+            return carry
+
+        lax.fori_loop(0, n_low, tell, 0)
+
 
     half = rows // 2
     pending = []
@@ -204,15 +231,14 @@
     def cum_copy(way, blk, k, to):
         return rdma(cum.at[blk], cum.at[blk], cum_send.at[way, k], cum_recv.at[blk], sp=to)
 
-    first_up = z < n - 1
-    first_down = z <= half_n - 2
-    for way, cond, to in ((0, first_up, up), (1, first_down, down)):
-
-        @pl.when(cond)
-        def _(way=way, to=to):
-            cum_copy(way, z, 0, to).start()
-            for q in range(CHUNKS):
-                kv_copy(way, z, q, 0, to).start()
+    first_up = z < last
+
+    @pl.when(first_up)
+    def _():
+        pl.semaphore_wait(up_ready, 1)
+        cum_copy(0, z, 0, up).start()
+        for q in range(CHUNKS):
+            kv_copy(0, z, q, 0, up).start()
 
     for copy in loads[5:8]:
         copy.wait()
@@ -230,33 +256,50 @@
     for h in range(heads):
         mine = (lane >= h * hd) & (lane < (h + 1) * hd)
         qs[pl.ds(h * rows, rows)] = jnp.where(mine, query.astype(F32), 0.0).astype(BF16)
-    m_ref[...] = jnp.full_like(m_ref, -1e30)
-    l_ref[...] = jnp.zeros_like(l_ref)
-    acc[...] = jnp.zeros_like(acc)
     halo_copy = rdma(glu_tail, halo, halo_sem.at[0], halo_sem.at[1], sp=up)
 
     @pl.when(first_up)
     def _():
         halo_copy.start()
 
-    piece = heads * rows // CHUNKS
-    per_head = rows // piece
-
-    def attend(q, blk, offset):
-        h = q // per_head
-        here = pl.ds(q * piece, piece)
-        s = dot(qs[here], kv[blk, :, :width], NT)
-        s = s + (cum[z, h : h + 1, 0:1] - cum[blk, h : h + 1, :])
-        q_pos = lax.broadcasted_iota(jnp.int32, s.shape, 0) + (q % per_head) * piece + offset
-        k_pos = lax.broadcasted_iota(jnp.int32, s.shape, 1)
-        s = jnp.where(k_pos <= q_pos, s, -1e30)
-        m_old = m_ref[here]
-        m_new = jnp.maximum(m_old, jnp.max(s, axis=1, keepdims=True))
-        fade = jnp.exp(m_old - m_new)
-        p = jnp.exp(s - m_new[:, :1])
-        l_ref[here] = l_ref[here] * fade + jnp.sum(p, axis=1, keepdims=True)
+    ones = jnp.ones((rows, width), BF16)
+
+    def attend(h, blocks, diagonal=False):
+        here = pl.ds(h * rows, rows)
+        q = qs[here]
+        scores = []
+        for blk in blocks:
+            s = dot(q, kv[blk, :, :width], NT)
+            s = s + (cum[z, h : h + 1, 0:1] - cum[blk, h : h + 1, :])
+            if diagonal:
+                q_pos = lax.broadcasted_iota(jnp.int32, s.shape, 0)
+                k_pos = lax.broadcasted_iota(jnp.int32, s.shape, 1)
+                s = jnp.where(k_pos <= q_pos, s, -1e30)
+            scores.append(s)
+        best = scores[0]
+        for s in scores[1:]:
+            best = jnp.maximum(best, s)
+        m_new = jnp.broadcast_to(jnp.max(best, axis=1, keepdims=True), (rows, width))
+        if not diagonal:
+            m_old = m_ref[here]
+            m_new = jnp.maximum(m_old, m_new)
         m_ref[here] = m_new
-        acc[here] = acc[here] * fade + dot(p.astype(BF16), kv[blk, :, width:], NN)
+        wide = jnp.concatenate([m_new] * (rows // width), axis=1)
+        out = None
+        for blk, s in zip(blocks, scores):
+            p = jnp.exp(s - wide).astype(BF16)
+            o = dot(p, jnp.concatenate([kv[blk, :, width:], ones], axis=1), NN)
+            out = o if out is None else out + o
+        if diagonal:
+            acc[here] = out[:, :width]
+            l_ref[here] = out[:, width:]
+        else:
+            fade = jnp.exp(m_old - m_new)
+            acc[here] = acc[here] * fade + out[:, :width]
+            l_ref[here] = l_ref[here] * fade + out[:, width:]
+
+    for h in range(heads):
+        attend(h, [z], diagonal=True)
 
     def convolve():
         loads[8].wait()
@@ -323,17 +366,17 @@
     def flows(s):
         cw_in = (z >= s) & (s <= half_n)
         cw_on = cw_in & (z < n - 1) & (s < half_n)
-        reach = (z + s <= half_n - 2) | (z + s >= n)
-        cc_in = reach & (s <= half_n - 1)
-        cc_on = cc_in & (s < half_n - 1)
+        cc_in = (z + s >= n) & (s <= n_low)
+        cc_on = cc_in & (s < n_low)
         return cw_in, cw_on, cc_in, cc_on
 
     def step(s, carry):
         cw_in, cw_on, cc_in, cc_on = flows(s)
         j_cw, j_cc = (z + n - s) % n, (z + s) % n
         b_cw, b_cc = (z + n - s + 1) % n, (z + s - 1) % n
-        use_cw = z >= s - 1
-        use_cc = (z + s - 1 >= n) & (s <= half_n)
+        two = (z + s - 1 >= n) & (s <= half_n) & (s > 1)
+        one = (z >= s - 1) & (s > 1) & jnp.logical_not(two)
+        every = CHUNKS // heads
         for q in range(CHUNKS):
             for way, arrives, goes, blk, to in (
                 (0, cw_in, cw_on, j_cw, up),
@@ -352,13 +395,15 @@
                         cum_copy(way, blk, s, to).start()
                     kv_copy(way, blk, q, s, to).start()
 
-            @pl.when(use_cw)
-            def _():
-                attend(q, b_cw, (s - 1) * rows)
-
-            @pl.when(use_cc)
-            def _():
-                attend(q, b_cc, n * rows)
+            if q % every == every - 1:
+
+                @pl.when(two)
+                def _():
+                    attend(q // every, [b_cw, b_cc])
+
+                @pl.when(one)
+                def _():
+                    attend(q // every, [b_cw])
 
         @pl.when(s == conv_at)
         def _():
@@ -412,6 +457,13 @@
             )
             copy.start()
             outs.append((i, copy))
+    @pl.when(is_low)
+    def _():
+        pl.semaphore_wait(far_ready, 1)
+        cum_copy(1, z, 0, last).start()
+        for q in range(CHUNKS):
+            kv_copy(1, z, q, 0, last).start()
+
     log_ref[...] = log_row.T[:heads] + (cum[z] - cum[z][:, 0:1])
     for i in range(OUT_CUTS):
         total = xout[i, x].astype(F32)
@@ -424,7 +476,7 @@
 
     for copy in pending:
         copy.wait_send()
-    for way, cond, to in ((0, first_up, up), (1, first_down, down)):
+    for way, cond, to in ((0, first_up, up), (1, is_low, last)):
 
         @pl.when(cond)
         def _(way=way, to=to):
@@ -521,6 +573,8 @@
             dma((2, half_n)),
             dma((n,)),
             dma((2,)),
+            pltpu.SemaphoreType.REGULAR,
+            pltpu.SemaphoreType.REGULAR,
             dma((n_tp,)),
             dma((n_tp,)),
             dma((OUT_CUTS,)),

time: 117 us -> 122 us (1.043)
  the two profiles are of different devices: /device:TPU:33 before, /device:TPU:1323 now
where the time goes in v2:
time: 122 us
  Pallas kernels  118 us (97%)
  local copies, waits for them, and re-layouts  3.44 us (3%)
    pallas_call x1, Pallas kernels, local(): pl.pallas_call(functools.partial(layer, n, n_tp), out_shape=(jax.ShapeDty...  118 us

profile of v2, /device:TPU:1323, one launch (start us, length us, event | category | flops | bytes accessed | tf_op | source)
XLA Modules:
  0.0 122.1 jit_solution(12322525239794643172)
XLA Ops:
  0.6 1.3 %reshape.10.gain_hbm = bf16[1,2048]{1,0:T(2,128)(2,1)} reshape(bf16[2048]{0:T(1024)(128)(2,1)} %param.13) | data formatting | bytes 8192 | tf_op jit(solution)/shard_map/reshape | solution.py:597
  1.9 118.0 %shard_map.131 = (bf16[32,2048]{1,0:T(8,128)(2,1)}, f32[2,256]{1,0:T(2,128)}) custom-call(bf16[256,256]{1,0:T(8,128)(2,1)} %x_hbm.1, bf16[1,2048]{1,0:T(2,128)(2,1)} %reshape.10.gain_hbm, bf16[128,2048]{1,0:T(8,128)(2,1)} %wci_hbm.1, bf16[128,2048]{1,0:T(8,128)(2,1)} %wcg_hbm.1, bf16[31,128]{1,0:T(8,128)(2,1)} %taps_hbm.1, bf16[1,128]{1,0:T(2,128)(2,1)} %bitcast.1, ...), custom_call_target="tpu_custom_call" | custom-call | tf_op jit(solution)/shard_map/pallas_call | solution.py:585
  119.9 0.0 copy-start
  119.9 1.6 %copy.16 = bf16[32,2048]{1,0:T(8,128)(2,1)} copy(bf16[32,2048]{1,0:T(8,128)(2,1)} %get-tuple-element.4) | data formatting | bytes 262144
  121.5 0.0 copy-done
  121.5 0.6 copy.17
Async XLA Ops:
  119.9 1.6 %copy-start = (f32[2,256]{1,0:T(2,128)S(1)}, f32[2,256]{1,0:T(2,128)}, u32[]{:S(2)}) copy-start(f32[2,256]{1,0:T(2,128)} %get-tuple-element.5) | copy-start | bytes 6148

commit v3 on v2

--- a/solution.py
+++ b/solution.py
@@ -10,7 +10,7 @@
 MESH = pl.DeviceIdType.MESH
 F32 = jnp.float32
 BF16 = jnp.bfloat16
-CHUNKS = 4
+CHUNKS = 8
 OUT_CUTS = 2
 NT = (((1,), (1,)), ((), ()))
 NN = (((1,), (0,)), ((), ()))
@@ -71,7 +71,6 @@
     cum_send,
     cum_recv,
     halo_sem,
-    up_ready,
     far_ready,
     st_send,
     st_recv,
@@ -125,33 +124,45 @@
     for k in range(1, n_tp):
         pl.semaphore_signal(barrier, inc=1, device_id={"tp": (t + k) % n_tp}, device_id_type=MESH)
     last = n - 1
-    n_low = half_n - 1
+    reach = half_n + 1
+    n_low = last - reach
+    express = n // 4 + 1
     is_low = z < n_low
-
-    @pl.when(z < last)
+    relays_down = z >= reach + 2
+
+    @pl.when(z > 0)
+    def _():
+        pl.semaphore_signal(barrier, inc=1, device_id={"sp": down}, device_id_type=MESH)
+
+    @pl.when((z >= reach + 1) & (z < last))
     def _():
         pl.semaphore_signal(barrier, inc=1, device_id={"sp": up}, device_id_type=MESH)
 
+    @pl.when(z == express)
+    def _():
+        pl.semaphore_signal(barrier, inc=1, device_id={"sp": 0}, device_id_type=MESH)
+
     @pl.when(is_low)
     def _():
         pl.semaphore_signal(barrier, inc=1, device_id={"sp": last}, device_id_type=MESH)
 
     pl.semaphore_wait(
-        barrier, n_tp - 1 + jnp.where(z > 0, 1, 0) + jnp.where(z == last, n_low, 0)
+        barrier,
+        n_tp
+        - 1
+        + jnp.where(z < last, 1, 0)
+        + jnp.where(relays_down, 1, 0)
+        + jnp.where(z == 0, 1, 0)
+        + jnp.where(z == last, n_low, 0),
     )
 
-    @pl.when(z > 0)
-    def _():
-        pl.semaphore_signal(up_ready, inc=1, device_id={"sp": down}, device_id_type=MESH)
+    def tell(j):
+        pl.semaphore_signal(far_ready, inc=1, device_id={"sp": j}, device_id_type=MESH)
 
     @pl.when(z == last)
     def _():
-        def tell(j, carry):
-            pl.semaphore_signal(far_ready, inc=1, device_id={"sp": j}, device_id_type=MESH)
-            return carry
-
-        lax.fori_loop(0, n_low, tell, 0)
-
+        for j in range(min(4, n_low)):
+            tell(j)
 
     half = rows // 2
     pending = []
@@ -235,7 +246,6 @@
 
     @pl.when(first_up)
     def _():
-        pl.semaphore_wait(up_ready, 1)
         cum_copy(0, z, 0, up).start()
         for q in range(CHUNKS):
             kv_copy(0, z, q, 0, up).start()
@@ -363,24 +373,50 @@
     conv_at = 2
     stats_at = min(5, half_n + 1)
 
-    def flows(s):
-        cw_in = (z >= s) & (s <= half_n)
-        cw_on = cw_in & (z < n - 1) & (s < half_n)
-        cc_in = (z + s >= n) & (s <= n_low)
-        cc_on = cc_in & (s < n_low)
-        return cw_in, cw_on, cc_in, cc_on
+    lag = jnp.maximum(last - z, 0) // 2
+
+    def flow_up(s):
+        comes = (z >= s) & (s <= reach)
+        goes = comes & (z < last) & (s < reach) & jnp.logical_not((z == s) & (z == express - 1))
+        return comes, goes
+
+    def flow_down(s):
+        comes = (s >= 1) & (z + s >= n) & (s <= n_low)
+        goes = comes & (s < n_low) & relays_down
+        return comes, goes
+
+    def send_far():
+        @pl.when(z == 0)
+        def _():
+            cum_copy(1, z, 1, express).start()
+            for q in range(CHUNKS):
+                kv_copy(1, z, q, 1, express).start()
+
+        pl.semaphore_wait(far_ready, 1)
+        cum_copy(1, z, 0, last).start()
+        for q in range(CHUNKS):
+            kv_copy(1, z, q, 0, last).start()
 
     def step(s, carry):
-        cw_in, cw_on, cc_in, cc_on = flows(s)
-        j_cw, j_cc = (z + n - s) % n, (z + s) % n
-        b_cw, b_cc = (z + n - s + 1) % n, (z + s - 1) % n
-        two = (z + s - 1 >= n) & (s <= half_n) & (s > 1)
-        one = (z >= s - 1) & (s > 1) & jnp.logical_not(two)
+        d = s - lag
+        cw_in, cw_on = flow_up(s)
+        cc_in, cc_on = flow_down(d)
+        j_cw, j_cc = (z + n - s) % n, (z + n + d) % n
+        b_cw, b_cc = (z + n - s + 1) % n, (z + n + d - 1) % n
+        has_cw = (z >= s - 1) & (s > 1) & (s - 1 <= reach)
+        has_cc, _ = flow_down(d - 1)
+        two = has_cw & has_cc
+        one = has_cw ^ has_cc
         every = CHUNKS // heads
+
+        @pl.when(is_low & (s == jnp.maximum(z, 1)))
+        def _():
+            send_far()
+
         for q in range(CHUNKS):
-            for way, arrives, goes, blk, to in (
-                (0, cw_in, cw_on, j_cw, up),
-                (1, cc_in, cc_on, j_cc, down),
+            for way, arrives, goes, blk, to, k in (
+                (0, cw_in, cw_on, j_cw, up, s),
+                (1, cc_in, cc_on, j_cc, down, d),
             ):
 
                 @pl.when(arrives)
@@ -390,10 +426,10 @@
                     kv_copy(way, blk, q, 0, to).wait_recv()
 
                 @pl.when(goes)
-                def _(way=way, blk=blk, to=to):
+                def _(way=way, blk=blk, to=to, k=k):
                     if q == 0:
-                        cum_copy(way, blk, s, to).start()
-                    kv_copy(way, blk, q, s, to).start()
+                        cum_copy(way, blk, k, to).start()
+                    kv_copy(way, blk, q, k, to).start()
 
             if q % every == every - 1:
 
@@ -403,7 +439,15 @@
 
                 @pl.when(one)
                 def _():
-                    attend(q // every, [b_cw])
+                    attend(q // every, [jnp.where(has_cw, b_cw, b_cc)])
+
+        @pl.when((z == last) & cc_in)
+        def _():
+            for j in (2 * s + 2, 2 * s + 3):
+
+                @pl.when(j < n_low)
+                def _(j=j):
+                    tell(j)
 
         @pl.when(s == conv_at)
         def _():
@@ -416,7 +460,7 @@
 
         return carry
 
-    lax.fori_loop(1, half_n + 2, step, 0)
+    lax.fori_loop(1, max(reach + 1, n_low + 1 + (n_low - 1) // 2) + 1, step, 0)
 
     tops, sums = m_ref[...], l_ref[...]
     logs = tops + jnp.log(sums)
@@ -457,13 +501,6 @@
             )
             copy.start()
             outs.append((i, copy))
-    @pl.when(is_low)
-    def _():
-        pl.semaphore_wait(far_ready, 1)
-        cum_copy(1, z, 0, last).start()
-        for q in range(CHUNKS):
-            kv_copy(1, z, q, 0, last).start()
-
     log_ref[...] = log_row.T[:heads] + (cum[z] - cum[z][:, 0:1])
     for i in range(OUT_CUTS):
         total = xout[i, x].astype(F32)
@@ -491,9 +528,17 @@
     for k in range(1, n_tp):
         stat_copy(k).wait_send()
 
+    @pl.when(z == 0)
+    def _():
+        cum_copy(1, z, 1, express).wait_send()
+        for q in range(CHUNKS):
+            kv_copy(1, z, q, 1, express).wait_send()
+
     def drain(s, carry):
-        cw_in, cw_on, cc_in, cc_on = flows(s)
-        for way, goes, blk, to in ((0, cw_on, (z + n - s) % n, up), (1, cc_on, (z + s) % n, down)):
+        for way, goes, blk, to in (
+            (0, flow_up(s)[1], (z + n - s) % n, up),
+            (1, flow_down(s)[1], (z + s) % n, down),
+        ):
 
             @pl.when(goes)
             def _(way=way, blk=blk, to=to):
@@ -503,7 +548,7 @@
 
         return carry
 
-    lax.fori_loop(1, half_n, drain, 0)
+    lax.fori_loop(1, reach, drain, 0)
     for copy in pairs:
         copy.wait_send()
     for k, copy in outs:
@@ -568,12 +613,11 @@
             dma((12,)),
             dma((14,)),
             dma((n_tp, 2)),
-            dma((2, half_n, CHUNKS)),
+            dma((2, half_n + 1, CHUNKS)),
             dma((n, CHUNKS)),
-            dma((2, half_n)),
+            dma((2, half_n + 1)),
             dma((n,)),
             dma((2,)),
-            pltpu.SemaphoreType.REGULAR,
             pltpu.SemaphoreType.REGULAR,
             dma((n_tp,)),
             dma((n_tp,)),

time: 122 us -> 110 us (0.902)
  the two profiles are of different devices: /device:TPU:1323 before, /device:TPU:1121 now
where the time goes in v3:
time: 110 us
  Pallas kernels  106 us (96%)
  local copies, waits for them, and re-layouts  3.44 us (3%)
    pallas_call x1, Pallas kernels, local(): pl.pallas_call(functools.partial(layer, n, n_tp), out_shape=(jax.ShapeDty...  106 us

profile of v3, /device:TPU:1121, one launch (start us, length us, event | category | flops | bytes accessed | tf_op | source)
XLA Modules:
  0.0 110.2 jit_solution(10578243643648555233)
XLA Ops:
  0.6 1.3 %reshape.10.gain_hbm = bf16[1,2048]{1,0:T(2,128)(2,1)} reshape(bf16[2048]{0:T(1024)(128)(2,1)} %param.13) | data formatting | bytes 8192 | tf_op jit(solution)/shard_map/reshape | solution.py:641
  1.9 106.1 %shard_map.131 = (bf16[32,2048]{1,0:T(8,128)(2,1)}, f32[2,256]{1,0:T(2,128)}) custom-call(bf16[256,256]{1,0:T(8,128)(2,1)} %x_hbm.1, bf16[1,2048]{1,0:T(2,128)(2,1)} %reshape.10.gain_hbm, bf16[128,2048]{1,0:T(8,128)(2,1)} %wci_hbm.1, bf16[128,2048]{1,0:T(8,128)(2,1)} %wcg_hbm.1, bf16[31,128]{1,0:T(8,128)(2,1)} %taps_hbm.1, bf16[1,128]{1,0:T(2,128)(2,1)} %bitcast.1, ...), custom_call_target="tpu_custom_call" | custom-call | tf_op jit(solution)/shard_map/pallas_call | solution.py:629
  108.1 0.0 copy-start
  108.1 1.6 %copy.16 = bf16[32,2048]{1,0:T(8,128)(2,1)} copy(bf16[32,2048]{1,0:T(8,128)(2,1)} %get-tuple-element.4) | data formatting | bytes 262144
  109.7 0.0 copy-done
  109.7 0.6 copy.17
Async XLA Ops:
  108.1 1.6 %copy-start = (f32[2,256]{1,0:T(2,128)S(1)}, f32[2,256]{1,0:T(2,128)}, u32[]{:S(2)}) copy-start(f32[2,256]{1,0:T(2,128)} %get-tuple-element.5) | copy-start | bytes 6148

commit v4 on v3

--- a/solution.py
+++ b/solution.py
@@ -10,7 +10,7 @@
 MESH = pl.DeviceIdType.MESH
 F32 = jnp.float32
 BF16 = jnp.bfloat16
-CHUNKS = 8
+CHUNKS = 4
 OUT_CUTS = 2
 NT = (((1,), (1,)), ((), ()))
 NN = (((1,), (0,)), ((), ()))
@@ -40,6 +40,7 @@
     xg,
     xs,
     gain,
+    gain32,
     taps,
     lng,
     wkv,
@@ -127,6 +128,7 @@
     reach = half_n + 1
     n_low = last - reach
     express = n // 4 + 1
+    first_tells = 4
     is_low = z < n_low
     relays_down = z >= reach + 2
 
@@ -161,7 +163,7 @@
 
     @pl.when(z == last)
     def _():
-        for j in range(min(4, n_low)):
+        for j in range(min(first_tells, n_low)):
             tell(j)
 
     half = rows // 2
@@ -188,6 +190,7 @@
     send_in(t, 1, mate)
     for copy in loads[1:4]:
         copy.wait()
+    gain32[...] = gain[...].astype(F32)
     kvacc[...] = jnp.zeros_like(kvacc)
     sq[...] = jnp.zeros_like(sq)
 
@@ -196,7 +199,8 @@
         lanes = pl.ds(pl.multiple_of(slot * feat, feat), feat)
         s2 = xf * xf
         sq[...] += s2[:, :128] + s2[:, 128:]
-        sc = (xf * gain[:, lanes].astype(F32)).astype(BF16)
+        scale = [gain32[pl.ds(slot * (feat // 128) + i, 1)] for i in range(feat // 128)]
+        sc = (xf * jnp.concatenate(scale, axis=1)).astype(BF16)
         xs[slot] = sc
         kvacc[...] += dot(sc, wkv[:, lanes], NT)
 
@@ -237,12 +241,17 @@
 
     def kv_copy(way, blk, q, k, to):
         ref = kv.at[blk, pl.ds(q * chunk, chunk)]
-        return rdma(ref, ref, kv_send.at[way, k, q], kv_recv.at[blk, q], sp=to)
+        return rdma(ref, ref, kv_send.at[way, k % 2, q], kv_recv.at[blk, q], sp=to)
 
     def cum_copy(way, blk, k, to):
-        return rdma(cum.at[blk], cum.at[blk], cum_send.at[way, k], cum_recv.at[blk], sp=to)
+        return rdma(cum.at[blk], cum.at[blk], cum_send.at[way, k % 2], cum_recv.at[blk], sp=to)
 
     first_up = z < last
+
+    @pl.when(z == last)
+    def _():
+        for j in range(first_tells, min(first_tells + 2, n_low)):
+            tell(j)
 
     @pl.when(first_up)
     def _():
@@ -409,14 +418,14 @@
         one = has_cw ^ has_cc
         every = CHUNKS // heads
 
-        @pl.when(is_low & (s == jnp.maximum(z, 1)))
+        @pl.when(is_low & (z < express) & (s == jnp.maximum(z, 1)))
         def _():
             send_far()
 
         for q in range(CHUNKS):
-            for way, arrives, goes, blk, to, k in (
-                (0, cw_in, cw_on, j_cw, up, s),
-                (1, cc_in, cc_on, j_cc, down, d),
+            for way, arrives, goes, blk, to, k, again in (
+                (0, cw_in, cw_on, j_cw, up, s, s >= 2),
+                (1, cc_in, cc_on, j_cc, down, d, d - 2 >= n - z),
             ):
 
                 @pl.when(arrives)
@@ -425,6 +434,12 @@
                         cum_copy(way, blk, 0, to).wait_recv()
                     kv_copy(way, blk, q, 0, to).wait_recv()
 
+                @pl.when(goes & again)
+                def _(way=way, blk=blk, to=to, k=k):
+                    if q == 0:
+                        cum_copy(way, blk, k, to).wait_send()
+                    kv_copy(way, blk, q, k, to).wait_send()
+
                 @pl.when(goes)
                 def _(way=way, blk=blk, to=to, k=k):
                     if q == 0:
@@ -441,11 +456,12 @@
                 def _():
                     attend(q // every, [jnp.where(has_cw, b_cw, b_cc)])
 
-        @pl.when((z == last) & cc_in)
+        @pl.when((z == last) & (s <= n_low))
         def _():
-            for j in (2 * s + 2, 2 * s + 3):
-
-                @pl.when(j < n_low)
+            first = first_tells + 2 + s + s // 2
+            for j, really in ((first - 1, s % 2 < 2), (first, s % 2 == 1)):
+
+                @pl.when(really & (j < n_low))
                 def _(j=j):
                     tell(j)
 
@@ -460,7 +476,12 @@
 
         return carry
 
-    lax.fori_loop(1, max(reach + 1, n_low + 1 + (n_low - 1) // 2) + 1, step, 0)
+    steps = jnp.where(
+        z > reach,
+        jnp.maximum(reach + 1, n_low + 1 + lag),
+        jnp.maximum(z + 1, stats_at),
+    )
+    lax.fori_loop(1, steps + 1, step, 0)
 
     tops, sums = m_ref[...], l_ref[...]
     logs = tops + jnp.log(sums)
@@ -501,6 +522,10 @@
             )
             copy.start()
             outs.append((i, copy))
+    @pl.when(is_low & (z >= express))
+    def _():
+        send_far()
+
     log_ref[...] = log_row.T[:heads] + (cum[z] - cum[z][:, 0:1])
     for i in range(OUT_CUTS):
         total = xout[i, x].astype(F32)
@@ -513,13 +538,20 @@
 
     for copy in pending:
         copy.wait_send()
-    for way, cond, to in ((0, first_up, up), (1, is_low, last)):
+    ups = jnp.minimum(z, reach - 1) - jnp.where(z == express - 1, 1, 0) + 1
+    downs = z - (reach + 1)
+    for way, parity, cond in (
+        (0, 0, first_up),
+        (0, 1, first_up & (ups > 1)),
+        (1, 0, is_low | (downs > 1) | ((downs == 1) & ((n_low - 1) % 2 == 0))),
+        (1, 1, (z == 0) | (downs > 1) | ((downs == 1) & ((n_low - 1) % 2 == 1))),
+    ):
 
         @pl.when(cond)
-        def _(way=way, to=to):
-            cum_copy(way, z, 0, to).wait_send()
+        def _(way=way, parity=parity):
+            cum_copy(way, z, parity, up).wait_send()
             for q in range(CHUNKS):
-                kv_copy(way, z, q, 0, to).wait_send()
+                kv_copy(way, z, q, parity, up).wait_send()
 
     @pl.when(first_up)
     def _():
@@ -528,27 +560,6 @@
     for k in range(1, n_tp):
         stat_copy(k).wait_send()
 
-    @pl.when(z == 0)
-    def _():
-        cum_copy(1, z, 1, express).wait_send()
-        for q in range(CHUNKS):
-            kv_copy(1, z, q, 1, express).wait_send()
-
-    def drain(s, carry):
-        for way, goes, blk, to in (
-            (0, flow_up(s)[1], (z + n - s) % n, up),
-            (1, flow_down(s)[1], (z + s) % n, down),
-        ):
-
-            @pl.when(goes)
-            def _(way=way, blk=blk, to=to):
-                cum_copy(way, blk, s, to).wait_send()
-                for q in range(CHUNKS):
-                    kv_copy(way, blk, q, s, to).wait_send()
-
-        return carry
-
-    lax.fori_loop(1, reach, drain, 0)
     for copy in pairs:
         copy.wait_send()
     for k, copy in outs:
@@ -586,7 +597,8 @@
         scratch = [
             vmem((n_tp, rows, feat), BF16),
             vmem((n_tp, rows, feat), BF16),
-            vmem((1, full), BF16),
+            vmem((full // 128, 128), BF16),
+            vmem((full // 128, 128), F32),
             vmem((n_taps, width), BF16),
             vmem((1, width), BF16),
             vmem((2 * width, full), BF16),
@@ -613,9 +625,9 @@
             dma((12,)),
             dma((14,)),
             dma((n_tp, 2)),
-            dma((2, half_n + 1, CHUNKS)),
+            dma((2, 2, CHUNKS)),
             dma((n, CHUNKS)),
-            dma((2, half_n + 1)),
+            dma((2, 2)),
             dma((n,)),
             dma((2,)),
             pltpu.SemaphoreType.REGULAR,
@@ -638,7 +650,7 @@
             compiler_params=pltpu.CompilerParams(collective_id=0, has_side_effects=True),
         )(
             inputs,
-            norm_gain.reshape(1, full),
+            norm_gain.reshape(full // 128, 128),
             w_conv_in,
             w_conv_gate,
             conv_kernel,

time: 110 us -> 89.5 us (0.81)
  the two profiles are of different devices: /device:TPU:1121 before, /device:TPU:1193 now
where the time goes in v4:
time: 89.5 us; the launch traced here: 89.4 us
  Pallas kernels  86.6 us (97%)
  local copies, waits for them, and re-layouts  2.15 us (2%)
    pallas_call x1, Pallas kernels, local(): pl.pallas_call(functools.partial(layer, n, n_tp), out_shape=(jax.ShapeDty...  86.6 us
    unnamed x4, local copies, waits for them, and re-layouts  2.15 us

profile of v4, /device:TPU:1193, one launch (start us, length us, event | category | flops | bytes accessed | tf_op | source)
XLA Modules:
  0.0 89.4 jit_solution(13822236272069708363)
XLA Ops:
  0.6 86.6 %shard_map.131 = (bf16[32,2048]{1,0:T(8,128)(2,1)}, f32[2,256]{1,0:T(2,128)}) custom-call(bf16[256,256]{1,0:T(8,128)(2,1)} %x_hbm.1, bf16[16,128]{1,0:T(8,128)(2,1)} %bitcast.2, bf16[128,2048]{1,0:T(8,128)(2,1)} %wci_hbm.1, bf16[128,2048]{1,0:T(8,128)(2,1)} %wcg_hbm.1, bf16[31,128]{1,0:T(8,128)(2,1)} %taps_hbm.1, bf16[1,128]{1,0:T(2,128)(2,1)} %bitcast.3, ...), custom_call_target="tpu_custom_call" | custom-call | tf_op jit(solution)/shard_map/pallas_call | solution.py:641
  87.2 0.0 copy-start
  87.2 1.6 %copy.16 = bf16[32,2048]{1,0:T(8,128)(2,1)} copy(bf16[32,2048]{1,0:T(8,128)(2,1)} %get-tuple-element.4) | data formatting | bytes 262144
  88.8 0.0 copy-done
  88.8 0.6 copy.17
Async XLA Ops:
  87.2 1.6 %copy-start = (f32[2,256]{1,0:T(2,128)S(1)}, f32[2,256]{1,0:T(2,128)}, u32[]{:S(2)}) copy-start(f32[2,256]{1,0:T(2,128)} %get-tuple-element.5) | copy-start | bytes 6148

commit v5 on v4

--- a/solution.py
+++ b/solution.py
@@ -35,8 +35,11 @@
     cum_hbm,
     wco_hbm,
     wao_hbm,
+    mixed_hbm,
+    log_hbm,
     mixed_ref,
     log_ref,
+    out_sem,
     xg,
     xs,
     gain,
@@ -125,18 +128,26 @@
     for k in range(1, n_tp):
         pl.semaphore_signal(barrier, inc=1, device_id={"tp": (t + k) % n_tp}, device_id_type=MESH)
     last = n - 1
-    reach = half_n + 1
-    n_low = last - reach
+    n_low = last - half_n
+
+    def lowest(p):
+        return jnp.where(
+            p <= half_n + 2,
+            0,
+            jnp.where(p <= half_n + 3, 1, p - half_n - jnp.where(p <= half_n + 8, 1, 0)),
+        )
+
+    low, low_up, low_down = lowest(z), lowest(z + 1), lowest(z - 1)
     express = n // 4 + 1
     first_tells = 4
     is_low = z < n_low
-    relays_down = z >= reach + 2
+    relays_down = low_down > 0
 
     @pl.when(z > 0)
     def _():
         pl.semaphore_signal(barrier, inc=1, device_id={"sp": down}, device_id_type=MESH)
 
-    @pl.when((z >= reach + 1) & (z < last))
+    @pl.when((low > 0) & (z < last))
     def _():
         pl.semaphore_signal(barrier, inc=1, device_id={"sp": up}, device_id_type=MESH)
 
@@ -166,28 +177,26 @@
         for j in range(min(first_tells, n_low)):
             tell(j)
 
-    half = rows // 2
+    quarter = rows // 4
     pending = []
 
-    def part(slot, h):
-        return xg.at[slot, pl.ds(h * half, half)]
-
-    def send_in(slot, h, to):
+    def part(slot, h, m=1):
+        return xg.at[slot, pl.ds(h * quarter, m * quarter)]
+
+    def send_in(slot, h, to, m=1):
         k = len(pending)
-        copy = rdma(part(slot, h), part(slot, h), in_send.at[k], in_recv.at[slot, h], tp=to)
+        copy = rdma(part(slot, h, m), part(slot, h, m), in_send.at[k], in_recv.at[slot, h], tp=to)
         copy.start()
         pending.append(copy)
 
-    def got(slot, h):
-        rdma(part(slot, h), part(slot, h), in_send.at[0], in_recv.at[slot, h], tp=mate).wait_recv()
+    def got(slot, h, m=1):
+        rdma(part(slot, h, m), part(slot, h, m), in_send.at[0], in_recv.at[slot, h], tp=mate).wait_recv()
 
     loads[0].wait()
-    send_in(t, 0, right)
-    send_in(t, 1, left)
-    send_in(t, 1, right)
-    send_in(t, 0, left)
-    send_in(t, 0, mate)
-    send_in(t, 1, mate)
+    for h in range(4):
+        send_in(t, h, right)
+        send_in(t, (h + 2) % 4, left)
+    send_in(t, 0, mate, 4)
     for copy in loads[1:4]:
         copy.wait()
     gain32[...] = gain[...].astype(F32)
@@ -205,32 +214,32 @@
         kvacc[...] += dot(sc, wkv[:, lanes], NT)
 
     process(t)
-    got(mate, 0)
-    got(mate, 1)
+    got(mate, 0, 4)
     process(mate)
-    got(left, 0)
-    send_in(left, 0, right)
-    send_in(left, 0, mate)
-    got(right, 1)
-    send_in(right, 1, left)
-    send_in(right, 1, mate)
-    got(left, 1)
-    send_in(left, 1, mate)
-    got(right, 0)
-    send_in(right, 0, mate)
+    for h in range(2):
+        got(left, h)
+        send_in(left, h, right)
+        got(right, 2 + h)
+        send_in(right, 2 + h, left)
+    send_in(left, 0, mate, 2)
+    send_in(right, 2, mate, 2)
+    for h in range(2):
+        got(left, 2 + h)
+        got(right, h)
+    send_in(left, 2, mate, 2)
+    send_in(right, 0, mate, 2)
     process(left)
     process(right)
     for slot in (at(-1, 1 - c), at(1, 1 - c)):
-        got(slot, 0)
-        got(slot, 1)
+        got(slot, 0, 2)
+        got(slot, 2, 2)
         process(slot)
-    got(far, 0)
-    send_in(far, 0, mate)
-    got(far, 1)
-    send_in(far, 1, mate)
+    for h in (0, 2, 1, 3):
+        got(far, h)
+        send_in(far, h, mate)
     process(far)
-    got(at(2, 1 - c), 0)
-    got(at(2, 1 - c), 1)
+    for h in (0, 2, 1, 3):
+        got(at(2, 1 - c), h)
     process(at(2, 1 - c))
 
     rms = lax.rsqrt(jnp.sum(sq[...], axis=1, keepdims=True) / (feat * n_tp) + 1e-06)
@@ -382,16 +391,18 @@
     conv_at = 2
     stats_at = min(5, half_n + 1)
 
-    lag = jnp.maximum(last - z, 0) // 2
+    lag = jnp.where(low > 0, (last - z) // 3, 0)
 
     def flow_up(s):
-        comes = (z >= s) & (s <= reach)
-        goes = comes & (z < last) & (s < reach) & jnp.logical_not((z == s) & (z == express - 1))
+        blk = z - s
+        comes = (s >= 1) & (blk >= low)
+        goes = comes & (z < last) & (blk >= low_up) & jnp.logical_not((blk == 0) & (z == express - 1))
         return comes, goes
 
-    def flow_down(s):
-        comes = (s >= 1) & (z + s >= n) & (s <= n_low)
-        goes = comes & (s < n_low) & relays_down
+    def flow_down(d):
+        blk = z + d - n
+        comes = (d >= 1) & (blk >= 0) & (blk < low)
+        goes = comes & (blk < low_down)
         return comes, goes
 
     def send_far():
@@ -412,7 +423,7 @@
         cc_in, cc_on = flow_down(d)
         j_cw, j_cc = (z + n - s) % n, (z + n + d) % n
         b_cw, b_cc = (z + n - s + 1) % n, (z + n + d - 1) % n
-        has_cw = (z >= s - 1) & (s > 1) & (s - 1 <= reach)
+        has_cw, _ = flow_up(s - 1)
         has_cc, _ = flow_down(d - 1)
         two = has_cw & has_cc
         one = has_cw ^ has_cc
@@ -424,8 +435,8 @@
 
         for q in range(CHUNKS):
             for way, arrives, goes, blk, to, k, again in (
+                (1, cc_in, cc_on, j_cc, down, d, d - 2 >= n - z),
                 (0, cw_in, cw_on, j_cw, up, s, s >= 2),
-                (1, cc_in, cc_on, j_cc, down, d, d - 2 >= n - z),
             ):
 
                 @pl.when(arrives)
@@ -476,10 +487,8 @@
 
         return carry
 
-    steps = jnp.where(
-        z > reach,
-        jnp.maximum(reach + 1, n_low + 1 + lag),
-        jnp.maximum(z + 1, stats_at),
+    steps = jnp.maximum(
+        jnp.maximum(z - low + 1, stats_at), jnp.where(low > 0, n - z + low + lag, 0)
     )
     lax.fori_loop(1, steps + 1, step, 0)
 
@@ -527,6 +536,8 @@
         send_far()
 
     log_ref[...] = log_row.T[:heads] + (cum[z] - cum[z][:, 0:1])
+    results = [pltpu.make_async_copy(log_ref, log_hbm, out_sem.at[OUT_CUTS])]
+    results[0].start()
     for i in range(OUT_CUTS):
         total = xout[i, x].astype(F32)
         for k, copy in outs:
@@ -534,17 +545,20 @@
                 copy.wait_recv()
         for dx in range(nx - 1):
             total = total + xin[i, dx].astype(F32)
-        mixed_ref[:, i * cut : (i + 1) * cut] = total.astype(BF16)
+        columns = pl.ds(i * cut, cut)
+        mixed_ref[:, columns] = total.astype(BF16)
+        results.append(pltpu.make_async_copy(mixed_ref.at[:, columns], mixed_hbm.at[:, columns], out_sem.at[i]))
+        results[-1].start()
 
     for copy in pending:
         copy.wait_send()
-    ups = jnp.minimum(z, reach - 1) - jnp.where(z == express - 1, 1, 0) + 1
-    downs = z - (reach + 1)
+    ups = z - low_up - jnp.where(z == express - 1, 1, 0) + 1
+    downs = low_down
     for way, parity, cond in (
         (0, 0, first_up),
         (0, 1, first_up & (ups > 1)),
-        (1, 0, is_low | (downs > 1) | ((downs == 1) & ((n_low - 1) % 2 == 0))),
-        (1, 1, (z == 0) | (downs > 1) | ((downs == 1) & ((n_low - 1) % 2 == 1))),
+        (1, 0, is_low | (downs > 1) | ((downs == 1) & ((n - z) % 2 == 0))),
+        (1, 1, (z == 0) | (downs > 1) | ((downs == 1) & ((n - z) % 2 == 1))),
     ):
 
         @pl.when(cond)
@@ -564,6 +578,8 @@
         copy.wait_send()
     for k, copy in outs:
         copy.wait_send()
+    for copy in results:
+        copy.wait()
 
 
 def solution(mesh):
@@ -595,6 +611,9 @@
         dma = pltpu.SemaphoreType.DMA
         vmem = pltpu.VMEM
         scratch = [
+            vmem((each, full), BF16),
+            vmem((heads, rows), F32),
+            dma((OUT_CUTS + 1,)),
             vmem((n_tp, rows, feat), BF16),
             vmem((n_tp, rows, feat), BF16),
             vmem((full // 128, 128), BF16),
@@ -623,8 +642,8 @@
             vmem((OUT_CUTS, nx, each, cut), BF16),
             vmem((OUT_CUTS, nx - 1, each, cut), BF16),
             dma((12,)),
-            dma((14,)),
-            dma((n_tp, 2)),
+            dma((21,)),
+            dma((n_tp, 4)),
             dma((2, 2, CHUNKS)),
             dma((n, CHUNKS)),
             dma((2, 2)),
@@ -645,7 +664,7 @@
                 jax.ShapeDtypeStruct((heads, rows), F32),
             ),
             in_specs=[pl.BlockSpec(memory_space=pl.ANY)] * 12,
-            out_specs=(pl.BlockSpec(memory_space=pltpu.VMEM), pl.BlockSpec(memory_space=pltpu.VMEM)),
+            out_specs=(pl.BlockSpec(memory_space=pl.ANY), pl.BlockSpec(memory_space=pl.ANY)),
             scratch_shapes=scratch,
             compiler_params=pltpu.CompilerParams(collective_id=0, has_side_effects=True),
         )(

time: 89.5 us -> 89.9 us (level)
  the two profiles are of different devices: /device:TPU:1193 before, /device:TPU:1577 now
where the time goes in v5:
time: 89.9 us; the launch traced here: 89.8 us
  Pallas kernels  87 us (97%)
  local copies, waits for them, and re-layouts  2.15 us (2%)
    pallas_call x1, Pallas kernels, local(): pl.pallas_call(functools.partial(layer, n, n_tp), out_shape=(jax.ShapeDty...  87 us
    unnamed x4, local copies, waits for them, and re-layouts  2.15 us

profile of v5, /device:TPU:1577, one launch (start us, length us, event | category | flops | bytes accessed | tf_op | source)
XLA Modules:
  0.0 89.8 jit_solution(8518869743424920994)
XLA Ops:
  0.6 87.0 %shard_map.131 = (bf16[32,2048]{1,0:T(8,128)(2,1)}, f32[2,256]{1,0:T(2,128)}) custom-call(bf16[256,256]{1,0:T(8,128)(2,1)} %x_hbm.1, bf16[16,128]{1,0:T(8,128)(2,1)} %bitcast.2, bf16[128,2048]{1,0:T(8,128)(2,1)} %wci_hbm.1, bf16[128,2048]{1,0:T(8,128)(2,1)} %wcg_hbm.1, bf16[31,128]{1,0:T(8,128)(2,1)} %taps_hbm.1, bf16[1,128]{1,0:T(2,128)(2,1)} %bitcast.3, ...), custom_call_target="tpu_custom_call" | custom-call | tf_op jit(solution)/shard_map/pallas_call | solution.py:660
  87.6 0.0 copy-start
  87.6 1.6 %copy.16 = bf16[32,2048]{1,0:T(8,128)(2,1)} copy(bf16[32,2048]{1,0:T(8,128)(2,1)} %get-tuple-element.4) | data formatting | bytes 262144
  89.2 0.0 copy-done
  89.2 0.6 copy.17
Async XLA Ops:
  87.6 1.6 %copy-start = (f32[2,256]{1,0:T(2,128)S(1)}, f32[2,256]{1,0:T(2,128)}, u32[]{:S(2)}) copy-start(f32[2,256]{1,0:T(2,128)} %get-tuple-element.5) | copy-start | bytes 6148

commit v6 on v5

--- a/solution.py
+++ b/solution.py
@@ -131,15 +131,12 @@
     n_low = last - half_n
 
     def lowest(p):
-        return jnp.where(
-            p <= half_n + 2,
-            0,
-            jnp.where(p <= half_n + 3, 1, p - half_n - jnp.where(p <= half_n + 8, 1, 0)),
-        )
+        over = jnp.where(p <= half_n + 5, 2, jnp.where(p <= half_n + 11, 1, 0))
+        return jnp.maximum(p - half_n - over, 0)
 
     low, low_up, low_down = lowest(z), lowest(z + 1), lowest(z - 1)
     express = n // 4 + 1
-    first_tells = 4
+    first_tells = 3
     is_low = z < n_low
     relays_down = low_down > 0
 
@@ -259,7 +256,7 @@
 
     @pl.when(z == last)
     def _():
-        for j in range(first_tells, min(first_tells + 2, n_low)):
+        for j in range(first_tells, min(first_tells + 3, n_low)):
             tell(j)
 
     @pl.when(first_up)
@@ -391,7 +388,7 @@
     conv_at = 2
     stats_at = min(5, half_n + 1)
 
-    lag = jnp.where(low > 0, (last - z) // 3, 0)
+    lag = jnp.where(low > 0, 1 + (2 * (last - z) + 2) // 5, 0)
 
     def flow_up(s):
         blk = z - s
@@ -469,7 +466,7 @@
 
         @pl.when((z == last) & (s <= n_low))
         def _():
-            first = first_tells + 2 + s + s // 2
+            first = first_tells + 3 + s + s // 2
             for j, really in ((first - 1, s % 2 < 2), (first, s % 2 == 1)):
 
                 @pl.when(really & (j < n_low))

time: 89.9 us -> 89.3 us (level)
  the two profiles are of different devices: /device:TPU:1577 before, /device:TPU:1449 now
where the time goes in v6:
time: 89.3 us; the launch traced here: 89.1 us
  Pallas kernels  86.3 us (97%)
  local copies, waits for them, and re-layouts  2.15 us (2%)
    pallas_call x1, Pallas kernels, local(): pl.pallas_call(functools.partial(layer, n, n_tp), out_shape=(jax.ShapeDty...  86.3 us
    unnamed x4, local copies, waits for them, and re-layouts  2.15 us

profile of v6, /device:TPU:1449, one launch (start us, length us, event | category | flops | bytes accessed | tf_op | source)
XLA Modules:
  0.0 89.1 jit_solution(3747846822155083102)
XLA Ops:
  0.6 86.3 %shard_map.131 = (bf16[32,2048]{1,0:T(8,128)(2,1)}, f32[2,256]{1,0:T(2,128)}) custom-call(bf16[256,256]{1,0:T(8,128)(2,1)} %x_hbm.1, bf16[16,128]{1,0:T(8,128)(2,1)} %bitcast.2, bf16[128,2048]{1,0:T(8,128)(2,1)} %wci_hbm.1, bf16[128,2048]{1,0:T(8,128)(2,1)} %wcg_hbm.1, bf16[31,128]{1,0:T(8,128)(2,1)} %taps_hbm.1, bf16[1,128]{1,0:T(2,128)(2,1)} %bitcast.3, ...), custom_call_target="tpu_custom_call" | custom-call | tf_op jit(solution)/shard_map/pallas_call | solution.py:657
  87.0 0.0 copy-start
  87.0 1.6 %copy.16 = bf16[32,2048]{1,0:T(8,128)(2,1)} copy(bf16[32,2048]{1,0:T(8,128)(2,1)} %get-tuple-element.4) | data formatting | bytes 262144
  88.5 0.0 copy-done
  88.5 0.6 copy.17
Async XLA Ops:
  87.0 1.6 %copy-start = (f32[2,256]{1,0:T(2,128)S(1)}, f32[2,256]{1,0:T(2,128)}, u32[]{:S(2)}) copy-start(f32[2,256]{1,0:T(2,128)} %get-tuple-element.5) | copy-start | bytes 6148

commit v7 on v6

--- a/solution.py
+++ b/solution.py
@@ -48,7 +48,8 @@
     lng,
     wkv,
     w3,
-    wo,
+    wc_all,
+    wa_all,
     kv,
     cum,
     kvacc,
@@ -62,11 +63,11 @@
     halo,
     ctr,
     stats,
-    comb,
-    pair_out,
-    pair_in,
-    xout,
-    xin,
+    conv_src,
+    conv_in,
+    attn_src,
+    attn_in,
+    conv_part,
     ld_sem,
     in_send,
     in_recv,
@@ -78,10 +79,12 @@
     far_ready,
     st_send,
     st_recv,
-    pair_send,
-    pair_recv,
-    x_send,
-    x_recv,
+    w_send,
+    w_recv,
+    conv_send,
+    conv_recv,
+    attn_send,
+    attn_recv,
 ):
     z = lax.axis_index("sp")
     t = lax.axis_index("tp")
@@ -117,8 +120,8 @@
         (wq_hbm, w3.at[pl.ds(2 * width, width)]),
         (taps_hbm, taps),
         (lng_hbm, lng),
-        (wco_hbm, wo.at[pl.ds(0, width)]),
-        (wao_hbm, wo.at[pl.ds(width, width)]),
+        (wco_hbm, wc_all.at[pl.ds(pl.multiple_of(t * width, width), width)]),
+        (wao_hbm, wa_all.at[pl.ds(pl.multiple_of(t * width, width), width)]),
     ]
     loads = [pltpu.make_async_copy(a, b, ld_sem.at[i]) for i, (a, b) in enumerate(loads)]
     for copy in loads:
@@ -264,6 +267,26 @@
         cum_copy(0, z, 0, up).start()
         for q in range(CHUNKS):
             kv_copy(0, z, q, 0, up).start()
+
+    def w_part(slot, h):
+        whole = wc_all if h == 0 else wa_all
+        return whole.at[pl.ds(pl.multiple_of(slot * width, width), width)]
+
+    w_routes = [(t, 0, right), (t, 1, left), (t, 1, right), (t, 0, left), (t, 0, mate), (t, 1, mate)]
+    w_routes += [(left, 0, right), (left, 0, mate), (right, 1, left), (right, 1, mate)]
+    w_routes += [(left, 1, mate), (right, 0, mate), (far, 0, mate), (far, 1, mate)]
+    w_copies = [
+        rdma(w_part(slot, h), w_part(slot, h), w_send.at[k], w_recv.at[slot, h], tp=to)
+        for k, (slot, h, to) in enumerate(w_routes)
+    ]
+
+    def got_w(slot, h):
+        rdma(w_part(slot, h), w_part(slot, h), w_send.at[0], w_recv.at[slot, h], tp=mate).wait_recv()
+
+    for copy in loads[10:12]:
+        copy.wait()
+    for copy in w_copies[:6]:
+        copy.start()
 
     for copy in loads[5:8]:
         copy.wait()
@@ -381,11 +404,29 @@
         y = ((ctr[...] - mean) * lax.rsqrt(var + 1e-05)).T
         y = y * lng[...].astype(F32)
         y = (y * jax.nn.sigmoid(y)).astype(BF16)
-        each = rows // n_tp
+        spread(y, conv_src, conv_in, conv_send, conv_recv)
+
+    each = rows // n_tp
+
+    def row_copy(k, src, dst, send, recv):
+        d = (t + k) % n_tp
+        return rdma(src.at[d], dst.at[t], send.at[k], recv.at[t], tp=d)
+
+    def spread(values, src, dst, send, recv):
         for d in range(n_tp):
-            comb[d // 2, d % 2, :, :width] = y[d * each : (d + 1) * each]
+            src[d] = values[d * each : (d + 1) * each]
+        for k in range(1, n_tp):
+            row_copy(k, src, dst, send, recv).start()
+        dst[t] = src[t]
+
+    def collect(src, dst, send, recv):
+        for k in range(1, n_tp):
+            d = (t + k) % n_tp
+            rdma(dst.at[d], dst.at[d], send.at[0], recv.at[d], tp=d).wait_recv()
+        return jnp.concatenate([dst[d] for d in range(n_tp)], axis=1)
 
     conv_at = 2
+    w_at = (6, 10, 14)
     stats_at = min(5, half_n + 1)
 
     lag = jnp.where(low > 0, 1 + (2 * (last - z) + 2) // 5, 0)
@@ -482,10 +523,33 @@
         def _():
             finish_conv()
 
+        @pl.when(s == w_at[0])
+        def _():
+            got_w(left, 0)
+            w_copies[6].start()
+            w_copies[7].start()
+            got_w(right, 1)
+            w_copies[8].start()
+            w_copies[9].start()
+
+        @pl.when(s == w_at[1])
+        def _():
+            got_w(left, 1)
+            w_copies[10].start()
+            got_w(right, 0)
+            w_copies[11].start()
+
+        @pl.when(s == w_at[2])
+        def _():
+            got_w(far, 0)
+            w_copies[12].start()
+            got_w(far, 1)
+            w_copies[13].start()
+
         return carry
 
     steps = jnp.maximum(
-        jnp.maximum(z - low + 1, stats_at), jnp.where(low > 0, n - z + low + lag, 0)
+        jnp.maximum(z - low + 1, max(stats_at, w_at[2])), jnp.where(low > 0, n - z + low + lag, 0)
     )
     lax.fori_loop(1, steps + 1, step, 0)
 
@@ -497,37 +561,8 @@
     for h in range(1, heads):
         attn_row = jnp.where(lane >= h * hd, attn[h * rows : (h + 1) * rows], attn_row)
         log_row = jnp.where(lane >= h, logs[h * rows : (h + 1) * rows], log_row)
-    each = rows // n_tp
-    attn_row = attn_row.astype(BF16)
-    for d in range(n_tp):
-        comb[d // 2, d % 2, :, width:] = attn_row[d * each : (d + 1) * each]
-
-    for copy in loads[10:12]:
-        copy.wait()
-    cut = wo.shape[1] // OUT_CUTS
-
-    def product(core, i):
-        lhs = comb[:, core].reshape(nx * each, 2 * width)
-        return dot(lhs, wo[:, i * cut : (i + 1) * cut], NN).reshape(nx, each, cut)
-
-    pairs = []
-    for i in range(OUT_CUTS):
-        pair_out[i] = product(1 - c, i).astype(BF16)
-        copy = rdma(pair_out.at[i], pair_in.at[i], pair_send.at[i], pair_recv.at[i], tp=mate)
-        copy.start()
-        pairs.append(copy)
-    outs = []
-    for i in range(OUT_CUTS):
-        own = product(c, i)
-        pairs[i].wait_recv()
-        xout[i] = (own + pair_in[i].astype(F32)).astype(BF16)
-        for dx in (2, 1, 3):
-            dst = at(dx - nx, c)
-            copy = rdma(
-                xout.at[i, (x + dx) % nx], xin.at[i, dx - 1], x_send.at[i, dx - 1], x_recv.at[i, dx - 1], tp=dst
-            )
-            copy.start()
-            outs.append((i, copy))
+    spread(attn_row.astype(BF16), attn_src, attn_in, attn_send, attn_recv)
+
     @pl.when(is_low & (z >= express))
     def _():
         send_far()
@@ -535,15 +570,18 @@
     log_ref[...] = log_row.T[:heads] + (cum[z] - cum[z][:, 0:1])
     results = [pltpu.make_async_copy(log_ref, log_hbm, out_sem.at[OUT_CUTS])]
     results[0].start()
+    for slot in (mate, at(-1, 1 - c), at(1, 1 - c), at(2, 1 - c)):
+        got_w(slot, 0)
+        got_w(slot, 1)
+    cut = wc_all.shape[1] // OUT_CUTS
+    lhs = collect(conv_src, conv_in, conv_send, conv_recv)
     for i in range(OUT_CUTS):
-        total = xout[i, x].astype(F32)
-        for k, copy in outs:
-            if k == i:
-                copy.wait_recv()
-        for dx in range(nx - 1):
-            total = total + xin[i, dx].astype(F32)
         columns = pl.ds(i * cut, cut)
-        mixed_ref[:, columns] = total.astype(BF16)
+        conv_part[:, columns] = dot(lhs, wc_all[:, columns], NN)
+    lhs = collect(attn_src, attn_in, attn_send, attn_recv)
+    for i in range(OUT_CUTS):
+        columns = pl.ds(i * cut, cut)
+        mixed_ref[:, columns] = (conv_part[:, columns] + dot(lhs, wa_all[:, columns], NN)).astype(BF16)
         results.append(pltpu.make_async_copy(mixed_ref.at[:, columns], mixed_hbm.at[:, columns], out_sem.at[i]))
         results[-1].start()
 
@@ -571,10 +609,11 @@
     for k in range(1, n_tp):
         stat_copy(k).wait_send()
 
-    for copy in pairs:
+    for copy in w_copies:
         copy.wait_send()
-    for k, copy in outs:
-        copy.wait_send()
+    for k in range(1, n_tp):
+        row_copy(k, conv_src, conv_in, conv_send, conv_recv).wait_send()
+        row_copy(k, attn_src, attn_in, attn_send, attn_recv).wait_send()
     for copy in results:
         copy.wait()
 
@@ -601,9 +640,7 @@
         heads = cum_gate.shape[0]
         n_taps = conv_kernel.shape[0]
         each = rows // n_tp
-        nx = n_tp // 2
         pad = 32
-        cut = full // OUT_CUTS
         half_n = n // 2
         dma = pltpu.SemaphoreType.DMA
         vmem = pltpu.VMEM
@@ -619,7 +656,8 @@
             vmem((1, width), BF16),
             vmem((2 * width, full), BF16),
             vmem((3 * width, full), BF16),
-            vmem((2 * width, full), BF16),
+            vmem((n_tp * width, full), BF16),
+            vmem((n_tp * width, full), BF16),
             vmem((n, rows, 2 * width), BF16),
             vmem((n, heads, rows), F32),
             vmem((rows, 2 * width), F32),
@@ -633,11 +671,11 @@
             vmem((pad, width), BF16),
             vmem((width, rows), F32),
             vmem((n_tp, 2, rows), F32),
-            vmem((nx, 2, each, 2 * width), BF16),
-            vmem((OUT_CUTS, nx, each, cut), BF16),
-            vmem((OUT_CUTS, nx, each, cut), BF16),
-            vmem((OUT_CUTS, nx, each, cut), BF16),
-            vmem((OUT_CUTS, nx - 1, each, cut), BF16),
+            vmem((n_tp, each, width), BF16),
+            vmem((n_tp, each, width), BF16),
+            vmem((n_tp, each, width), BF16),
+            vmem((n_tp, each, width), BF16),
+            vmem((each, full), F32),
             dma((12,)),
             dma((21,)),
             dma((n_tp, 4)),
@@ -649,10 +687,12 @@
             pltpu.SemaphoreType.REGULAR,
             dma((n_tp,)),
             dma((n_tp,)),
-            dma((OUT_CUTS,)),
-            dma((OUT_CUTS,)),
-            dma((OUT_CUTS, nx - 1)),
-            dma((OUT_CUTS, nx - 1)),
+            dma((14,)),
+            dma((n_tp, 2)),
+            dma((n_tp,)),
+            dma((n_tp,)),
+            dma((n_tp,)),
+            dma((n_tp,)),
         ]
         return pl.pallas_call(
             functools.partial(layer, n, n_tp),

time: 89.3 us -> 103 us (1.15)
  the two profiles are of different devices: /device:TPU:1449 before, /device:TPU:33 now
where the time goes in v7:
time: 103 us
  Pallas kernels  101 us (98%)
  local copies, waits for them, and re-layouts  2.15 us (2%)
    pallas_call x1, Pallas kernels, local(): pl.pallas_call(functools.partial(layer, n, n_tp), out_shape=(jax.ShapeDty...  101 us
    unnamed x4, local copies, waits for them, and re-layouts  2.15 us

profile of v7, /device:TPU:33, one launch (start us, length us, event | category | flops | bytes accessed | tf_op | source)
XLA Modules:
  0.0 103.3 jit_solution(1775885069134479367)
XLA Ops:
  0.6 100.5 %shard_map.131 = (bf16[32,2048]{1,0:T(8,128)(2,1)}, f32[2,256]{1,0:T(2,128)}) custom-call(bf16[256,256]{1,0:T(8,128)(2,1)} %x_hbm.1, bf16[16,128]{1,0:T(8,128)(2,1)} %bitcast.2, bf16[128,2048]{1,0:T(8,128)(2,1)} %wci_hbm.1, bf16[128,2048]{1,0:T(8,128)(2,1)} %wcg_hbm.1, bf16[31,128]{1,0:T(8,128)(2,1)} %taps_hbm.1, bf16[1,128]{1,0:T(2,128)(2,1)} %bitcast.3, ...), custom_call_target="tpu_custom_call" | custom-call | tf_op jit(solution)/shard_map/pallas_call | solution.py:697
  101.2 0.0 copy-start
  101.2 1.6 %copy.16 = bf16[32,2048]{1,0:T(8,128)(2,1)} copy(bf16[32,2048]{1,0:T(8,128)(2,1)} %get-tuple-element.4) | data formatting | bytes 262144
  102.8 0.0 copy-done
  102.8 0.6 copy.17
Async XLA Ops:
  101.2 1.6 %copy-start = (f32[2,256]{1,0:T(2,128)S(1)}, f32[2,256]{1,0:T(2,128)}, u32[]{:S(2)}) copy-start(f32[2,256]{1,0:T(2,128)} %get-tuple-element.5) | copy-start | bytes 6148

commit v8 on v7

--- a/solution.py
+++ b/solution.py
@@ -79,6 +79,14 @@
     far_ready,
     st_send,
     st_recv,
+    pair_out,
+    pair_in,
+    xout,
+    xin,
+    pair_send,
+    pair_recv,
+    x_send,
+    x_recv,
     w_send,
     w_recv,
     conv_send,
@@ -285,8 +293,10 @@
 
     for copy in loads[10:12]:
         copy.wait()
-    for copy in w_copies[:6]:
-        copy.start()
+    @pl.when(z > 0)
+    def _():
+        for copy in w_copies[:6]:
+            copy.start()
 
     for copy in loads[5:8]:
         copy.wait()
@@ -404,7 +414,11 @@
         y = ((ctr[...] - mean) * lax.rsqrt(var + 1e-05)).T
         y = y * lng[...].astype(F32)
         y = (y * jax.nn.sigmoid(y)).astype(BF16)
-        spread(y, conv_src, conv_in, conv_send, conv_recv)
+        split(y, conv_src)
+
+        @pl.when(z > 0)
+        def _():
+            spread(conv_src, conv_in, conv_send, conv_recv)
 
     each = rows // n_tp
 
@@ -412,9 +426,11 @@
         d = (t + k) % n_tp
         return rdma(src.at[d], dst.at[t], send.at[k], recv.at[t], tp=d)
 
-    def spread(values, src, dst, send, recv):
+    def split(values, src):
         for d in range(n_tp):
             src[d] = values[d * each : (d + 1) * each]
+
+    def spread(src, dst, send, recv):
         for k in range(1, n_tp):
             row_copy(k, src, dst, send, recv).start()
         dst[t] = src[t]
@@ -427,7 +443,7 @@
 
     conv_at = 2
     w_at = (6, 10, 14)
-    stats_at = min(5, half_n + 1)
+    stats_at = 12
 
     lag = jnp.where(low > 0, 1 + (2 * (last - z) + 2) // 5, 0)
 
@@ -523,7 +539,7 @@
         def _():
             finish_conv()
 
-        @pl.when(s == w_at[0])
+        @pl.when((z > 0) & (s == w_at[0]))
         def _():
             got_w(left, 0)
             w_copies[6].start()
@@ -532,14 +548,14 @@
             w_copies[8].start()
             w_copies[9].start()
 
-        @pl.when(s == w_at[1])
+        @pl.when((z > 0) & (s == w_at[1]))
         def _():
             got_w(left, 1)
             w_copies[10].start()
             got_w(right, 0)
             w_copies[11].start()
 
-        @pl.when(s == w_at[2])
+        @pl.when((z > 0) & (s == w_at[2]))
         def _():
             got_w(far, 0)
             w_copies[12].start()
@@ -561,7 +577,21 @@
     for h in range(1, heads):
         attn_row = jnp.where(lane >= h * hd, attn[h * rows : (h + 1) * rows], attn_row)
         log_row = jnp.where(lane >= h, logs[h * rows : (h + 1) * rows], log_row)
-    spread(attn_row.astype(BF16), attn_src, attn_in, attn_send, attn_recv)
+    split(attn_row.astype(BF16), attn_src)
+    cut = wc_all.shape[1] // OUT_CUTS
+    nx = n_tp // 2
+    own_rows = pl.ds(pl.multiple_of(t * width, width), width)
+
+    def product(core, i):
+        columns = slice(i * cut, (i + 1) * cut)
+        conv = jnp.concatenate([conv_src[2 * k + core] for k in range(nx)], axis=0)
+        attn = jnp.concatenate([attn_src[2 * k + core] for k in range(nx)], axis=0)
+        total = dot(conv, wc_all[own_rows, columns], NN) + dot(attn, wa_all[own_rows, columns], NN)
+        return total.reshape(nx, each, cut)
+
+    @pl.when(z > 0)
+    def _():
+        spread(attn_src, attn_in, attn_send, attn_recv)
 
     @pl.when(is_low & (z >= express))
     def _():
@@ -570,20 +600,54 @@
     log_ref[...] = log_row.T[:heads] + (cum[z] - cum[z][:, 0:1])
     results = [pltpu.make_async_copy(log_ref, log_hbm, out_sem.at[OUT_CUTS])]
     results[0].start()
-    for slot in (mate, at(-1, 1 - c), at(1, 1 - c), at(2, 1 - c)):
-        got_w(slot, 0)
-        got_w(slot, 1)
-    cut = wc_all.shape[1] // OUT_CUTS
-    lhs = collect(conv_src, conv_in, conv_send, conv_recv)
-    for i in range(OUT_CUTS):
-        columns = pl.ds(i * cut, cut)
-        conv_part[:, columns] = dot(lhs, wc_all[:, columns], NN)
-    lhs = collect(attn_src, attn_in, attn_send, attn_recv)
-    for i in range(OUT_CUTS):
-        columns = pl.ds(i * cut, cut)
-        mixed_ref[:, columns] = (conv_part[:, columns] + dot(lhs, wa_all[:, columns], NN)).astype(BF16)
-        results.append(pltpu.make_async_copy(mixed_ref.at[:, columns], mixed_hbm.at[:, columns], out_sem.at[i]))
-        results[-1].start()
+    @pl.when(z > 0)
+    def _():
+        for slot in (mate, at(-1, 1 - c), at(1, 1 - c), at(2, 1 - c)):
+            got_w(slot, 0)
+            got_w(slot, 1)
+        lhs = collect(conv_src, conv_in, conv_send, conv_recv)
+        for i in range(OUT_CUTS):
+            columns = pl.ds(i * cut, cut)
+            conv_part[:, columns] = dot(lhs, wc_all[:, columns], NN)
+        lhs = collect(attn_src, attn_in, attn_send, attn_recv)
+        for i in range(OUT_CUTS):
+            columns = pl.ds(i * cut, cut)
+            mixed_ref[:, columns] = (conv_part[:, columns] + dot(lhs, wa_all[:, columns], NN)).astype(BF16)
+
+    @pl.when(z == 0)
+    def _():
+        pairs = []
+        for i in range(OUT_CUTS):
+            pair_out[i] = product(1 - c, i).astype(BF16)
+            copy = rdma(pair_out.at[i], pair_in.at[i], pair_send.at[i], pair_recv.at[i], tp=mate)
+            copy.start()
+            pairs.append(copy)
+        outs = []
+        for i in range(OUT_CUTS):
+            own = product(c, i)
+            pairs[i].wait_recv()
+            xout[i] = (own + pair_in[i].astype(F32)).astype(BF16)
+            for dx in (2, 1, 3):
+                copy = rdma(
+                    xout.at[i, (x + dx) % nx], xin.at[i, dx - 1], x_send.at[i, dx - 1], x_recv.at[i, dx - 1], tp=at(dx - nx, c)
+                )
+                copy.start()
+                outs.append((i, copy))
+        for i in range(OUT_CUTS):
+            total = xout[i, x].astype(F32)
+            for k, copy in outs:
+                if k == i:
+                    copy.wait_recv()
+            for dx in range(nx - 1):
+                total = total + xin[i, dx].astype(F32)
+            mixed_ref[:, i * cut : (i + 1) * cut] = total.astype(BF16)
+        for copy in pairs:
+            copy.wait_send()
+        for k, copy in outs:
+            copy.wait_send()
+
+    results.append(pltpu.make_async_copy(mixed_ref, mixed_hbm, out_sem.at[0]))
+    results[-1].start()
 
     for copy in pending:
         copy.wait_send()
@@ -609,11 +673,14 @@
     for k in range(1, n_tp):
         stat_copy(k).wait_send()
 
-    for copy in w_copies:
-        copy.wait_send()
-    for k in range(1, n_tp):
-        row_copy(k, conv_src, conv_in, conv_send, conv_recv).wait_send()
-        row_copy(k, attn_src, attn_in, attn_send, attn_recv).wait_send()
+    @pl.when(z > 0)
+    def _():
+        for copy in w_copies:
+            copy.wait_send()
+        for k in range(1, n_tp):
+            row_copy(k, conv_src, conv_in, conv_send, conv_recv).wait_send()
+            row_copy(k, attn_src, attn_in, attn_send, attn_recv).wait_send()
+
     for copy in results:
         copy.wait()
 
@@ -687,6 +754,14 @@
             pltpu.SemaphoreType.REGULAR,
             dma((n_tp,)),
             dma((n_tp,)),
+            vmem((OUT_CUTS, n_tp // 2, each, full // OUT_CUTS), BF16),
+            vmem((OUT_CUTS, n_tp // 2, each, full // OUT_CUTS), BF16),
+            vmem((OUT_CUTS, n_tp // 2, each, full // OUT_CUTS), BF16),
+            vmem((OUT_CUTS, n_tp // 2 - 1, each, full // OUT_CUTS), BF16),
+            dma((OUT_CUTS,)),
+            dma((OUT_CUTS,)),
+            dma((OUT_CUTS, n_tp // 2 - 1)),
+            dma((OUT_CUTS, n_tp // 2 - 1)),
             dma((14,)),
             dma((n_tp, 2)),
             dma((n_tp,)),

time: 103 us -> 87.7 us (0.85)
  the two profiles are of different devices: /device:TPU:33 before, /device:TPU:353 now
where the time goes in v8:
time: 87.7 us; the launch traced here: 87.6 us
  Pallas kernels  84.8 us (97%)
  local copies, waits for them, and re-layouts  2.15 us (2%)
    pallas_call x1, Pallas kernels, local(): pl.pallas_call(functools.partial(layer, n, n_tp), out_shape=(jax.ShapeDty...  84.8 us
    unnamed x4, local copies, waits for them, and re-layouts  2.15 us

profile of v8, /device:TPU:353, one launch (start us, length us, event | category | flops | bytes accessed | tf_op | source)
XLA Modules:
  0.0 87.6 jit_solution(5084697609915737355)
XLA Ops:
  0.6 84.8 %shard_map.131 = (bf16[32,2048]{1,0:T(8,128)(2,1)}, f32[2,256]{1,0:T(2,128)}) custom-call(bf16[256,256]{1,0:T(8,128)(2,1)} %x_hbm.1, bf16[16,128]{1,0:T(8,128)(2,1)} %bitcast.2, bf16[128,2048]{1,0:T(8,128)(2,1)} %wci_hbm.1, bf16[128,2048]{1,0:T(8,128)(2,1)} %wcg_hbm.1, bf16[31,128]{1,0:T(8,128)(2,1)} %taps_hbm.1, bf16[1,128]{1,0:T(2,128)(2,1)} %bitcast.3, ...), custom_call_target="tpu_custom_call" | custom-call | tf_op jit(solution)/shard_map/pallas_call | solution.py:772
  85.4 0.0 copy-start
  85.4 1.6 %copy.16 = bf16[32,2048]{1,0:T(8,128)(2,1)} copy(bf16[32,2048]{1,0:T(8,128)(2,1)} %get-tuple-element.4) | data formatting | bytes 262144
  87.0 0.0 copy-done
  87.0 0.6 copy.17
Async XLA Ops:
  85.4 1.6 %copy-start = (f32[2,256]{1,0:T(2,128)S(1)}, f32[2,256]{1,0:T(2,128)}, u32[]{:S(2)}) copy-start(f32[2,256]{1,0:T(2,128)} %get-tuple-element.5) | copy-start | bytes 6148

commit v9 on v8

--- a/solution.py
+++ b/solution.py
@@ -147,7 +147,7 @@
 
     low, low_up, low_down = lowest(z), lowest(z + 1), lowest(z - 1)
     express = n // 4 + 1
-    first_tells = 3
+    first_tells = 4
     is_low = z < n_low
     relays_down = low_down > 0
 
@@ -267,7 +267,7 @@
 
     @pl.when(z == last)
     def _():
-        for j in range(first_tells, min(first_tells + 3, n_low)):
+        for j in range(first_tells, min(first_tells + 2, n_low)):
             tell(j)
 
     @pl.when(first_up)
@@ -523,7 +523,7 @@
 
         @pl.when((z == last) & (s <= n_low))
         def _():
-            first = first_tells + 3 + s + s // 2
+            first = first_tells + 2 + s + s // 2
             for j, really in ((first - 1, s % 2 < 2), (first, s % 2 == 1)):
 
                 @pl.when(really & (j < n_low))

time: 87.7 us -> 87.7 us (level)
  no operation moved by 1% of the time
where the time goes in v9:
time: 87.7 us; the launch traced here: 87.6 us
  Pallas kernels  84.8 us (97%)
  local copies, waits for them, and re-layouts  2.15 us (2%)
    pallas_call x1, Pallas kernels, local(): pl.pallas_call(functools.partial(layer, n, n_tp), out_shape=(jax.ShapeDty...  84.8 us
    unnamed x4, local copies, waits for them, and re-layouts  2.15 us

profile of v9, /device:TPU:353, one launch (start us, length us, event | category | flops | bytes accessed | tf_op | source)
XLA Modules:
  0.0 87.6 jit_solution(6177175661430389854)
XLA Ops:
  0.6 84.8 %shard_map.131 = (bf16[32,2048]{1,0:T(8,128)(2,1)}, f32[2,256]{1,0:T(2,128)}) custom-call(bf16[256,256]{1,0:T(8,128)(2,1)} %x_hbm.1, bf16[16,128]{1,0:T(8,128)(2,1)} %bitcast.2, bf16[128,2048]{1,0:T(8,128)(2,1)} %wci_hbm.1, bf16[128,2048]{1,0:T(8,128)(2,1)} %wcg_hbm.1, bf16[31,128]{1,0:T(8,128)(2,1)} %taps_hbm.1, bf16[1,128]{1,0:T(2,128)(2,1)} %bitcast.3, ...), custom_call_target="tpu_custom_call" | custom-call | tf_op jit(solution)/shard_map/pallas_call | solution.py:772
  85.4 0.0 copy-start
  85.4 1.6 %copy.16 = bf16[32,2048]{1,0:T(8,128)(2,1)} copy(bf16[32,2048]{1,0:T(8,128)(2,1)} %get-tuple-element.4) | data formatting | bytes 262144
  87.0 0.0 copy-done
  87.0 0.6 copy.17
Async XLA Ops:
  85.4 1.6 %copy-start = (f32[2,256]{1,0:T(2,128)S(1)}, f32[2,256]{1,0:T(2,128)}, u32[]{:S(2)}) copy-start(f32[2,256]{1,0:T(2,128)} %get-tuple-element.5) | copy-start | bytes 6148
